TPU v7x, 32 devices: a whole 2x2x4 slice. The times are simulated.
32 devices in a mesh: fs: 8 (over z, core), tp: 4 (over y, x).
Axes of the slice: x: 2, y: 2, z: 4, core: 2. Of those that a mesh axis runs over, the one named last changes fastest.
Arguments:
- late_input: bfloat16 [1024, 2048], P('fs'), may hold values from -6 to 6
- early_input: bfloat16 [1024, 2048], P('fs'), may hold values from -6 to 6
- early_mid: bfloat16 [1024, 2048], P('fs'), may hold values from -6 to 6
- cotangent: bfloat16 [1024, 2048], P('fs'), may hold values from -6 to 6
- gain_first: float32 [2048], replicated, may hold values from 0.1 to 1.9
- gain_second: float32 [2048], replicated, may hold values from 0.1 to 1.9
- gate_first: bfloat16 [2048, 2816], P('fs', 'tp'), may hold values from -0.125 to 0.125
- up_first: bfloat16 [2048, 2816], P('fs', 'tp'), may hold values from -0.125 to 0.125
- down_first: bfloat16 [2816, 2048], P('tp', 'fs'), may hold values from -0.109375 to 0.109375
- gate_second: bfloat16 [2048, 2816], P('fs', 'tp'), may hold values from -0.125 to 0.125
- up_second: bfloat16 [2048, 2816], P('fs', 'tp'), may hold values from -0.125 to 0.125
- down_second: bfloat16 [2816, 2048], P('tp', 'fs'), may hold values from -0.109375 to 0.109375
- sum_gate_first: float32 [2048, 2816], P('fs', 'tp'), may hold values from -128 to 128
- sum_up_first: float32 [2048, 2816], P('fs', 'tp'), may hold values from -128 to 128
- sum_down_first: float32 [2816, 2048], P('tp', 'fs'), may hold values from -128 to 128
- sum_gate_second: float32 [2048, 2816], P('fs', 'tp'), may hold values from -128 to 128
- sum_up_second: float32 [2048, 2816], P('fs', 'tp'), may hold values from -128 to 128
- sum_down_second: float32 [2816, 2048], P('tp', 'fs'), may hold values from -128 to 128
Outputs:
- late_mid: bfloat16 [1024, 2048], P('fs')
- late_out: bfloat16 [1024, 2048], P('fs')
- input_grad: bfloat16 [1024, 2048], P('fs')
- new_gate_first: float32 [2048, 2816], P('fs', 'tp')
- new_up_first: float32 [2048, 2816], P('fs', 'tp')
- new_down_first: float32 [2816, 2048], P('tp', 'fs')
- new_gate_second: float32 [2048, 2816], P('fs', 'tp')
- new_up_second: float32 [2048, 2816], P('fs', 'tp')
- new_down_second: float32 [2816, 2048], P('tp', 'fs')
All inputs are finite; a program needn't handle non-finite values.
Results may differ from a plain program's by a relative error of at most 0.015.
Values may be sent and summed in bfloat16 or wider, within the bound.
A program may use at most 128 MiB of HBM per device.

v0:
```python
import jax
import jax.numpy as jnp
from jax import lax
from jax.sharding import PartitionSpec as P

norm_eps = 1e-06


def normalize(values, gain_vector):
    widened = values.astype(jnp.float32)
    factor = lax.rsqrt(jnp.mean(widened * widened, axis=-1, keepdims=True) + norm_eps)
    normed = (widened * factor * gain_vector).astype(jnp.bfloat16)
    return (widened, factor, normed)


def project(rows, weights):
    return jnp.dot(rows, weights, preferred_element_type=jnp.float32)


def project_back(hidden_rows, weights):
    return jnp.einsum("tf,df->td", hidden_rows, weights, preferred_element_type=jnp.float32)


def fold_rows(left, right):
    return jnp.einsum("ta,tb->ab", left, right, preferred_element_type=jnp.float32)


def own_rows(rows):
    count = rows.shape[0] // lax.axis_size("tp")
    return lax.dynamic_slice_in_dim(rows, lax.axis_index("tp") * count, count, axis=0)


def sum_rows(partial):
    shares = lax.all_to_all(
        partial.astype(jnp.bfloat16), "tp", split_axis=0, concat_axis=0, tiled=True
    )
    shares = shares.reshape((lax.axis_size("tp"), -1, shares.shape[1]))
    return jnp.sum(shares.astype(jnp.float32), axis=0)


def join_rows(rows):
    return lax.all_gather(rows, "tp", axis=0, tiled=True)


def block_forward(values, gain_vector, weights, width):
    widened, factor, normed = normalize(values, gain_vector)
    pre = project(normed, weights[:, : 2 * width])
    hidden = (jax.nn.silu(pre[:, :width]) * pre[:, width:]).astype(jnp.bfloat16)
    branch = sum_rows(project_back(hidden, weights[:, 2 * width :]))
    return join_rows((own_rows(widened) + 0.5 * branch).astype(jnp.bfloat16))


def block_backward(normalized, cotangent, weights, width):
    widened, factor, normed = normalized
    pre = project(normed, weights[:, : 2 * width])
    gate_pre, up_pre = pre[:, :width], pre[:, width:]
    sigmoid_gate = jax.nn.sigmoid(gate_pre)
    activated = gate_pre * sigmoid_gate
    hidden = (activated * up_pre).astype(jnp.bfloat16)
    hidden_grad = 0.5 * project(cotangent, weights[:, 2 * width :])
    gate_grad = (
        hidden_grad * up_pre * sigmoid_gate * (1.0 + gate_pre * (1.0 - sigmoid_gate))
    ).astype(jnp.bfloat16)
    up_grad = (hidden_grad * activated).astype(jnp.bfloat16)
    pieces = jnp.concatenate((gate_grad, up_grad, hidden), axis=1)
    partial_value = project_back(pieces[:, : 2 * width], weights[:, : 2 * width])
    return (partial_value, pieces)


def backward_rows(normalized, cotangent, gain_vector, partial_value):
    normed_grad = sum_rows(partial_value)
    widened, factor = own_rows(normalized[0]), own_rows(normalized[1])
    scaled = normed_grad * gain_vector
    unit_rows = widened * factor
    rows_grad = own_rows(cotangent).astype(jnp.float32) + factor * (
        scaled - unit_rows * jnp.mean(scaled * unit_rows, axis=-1, keepdims=True)
    )
    return rows_grad.astype(jnp.bfloat16)


def gather_weights(gate, up, down):
    return lax.all_gather(jnp.concatenate((gate, up, down.T), axis=1), "fs", axis=0, tiled=True)


def share_columns(rows):
    return lax.all_to_all(rows, "fs", split_axis=1, concat_axis=0, tiled=True)


def join_columns(share):
    joined = join_rows(share)
    parts = joined.reshape((lax.axis_size("tp"), lax.axis_size("fs"), -1, joined.shape[1]))
    return jnp.swapaxes(parts, 0, 1).reshape(joined.shape)


def per_device(
    late_input,
    early_input,
    early_mid,
    cotangent,
    gain_first,
    gain_second,
    gate_first,
    up_first,
    down_first,
    gate_second,
    up_second,
    down_second,
    sum_gate_first,
    sum_up_first,
    sum_down_first,
    sum_gate_second,
    sum_up_second,
    sum_down_second,
):
    width = gate_first.shape[1]
    weights_second = gather_weights(gate_second, up_second, down_second)
    weights_first = gather_weights(gate_first, up_first, down_first)
    norm_second = normalize(early_mid, gain_second)
    norm_first = normalize(early_input, gain_first)
    early_rows = jnp.stack(
        (own_rows(norm_second[2]), own_rows(norm_first[2]), own_rows(cotangent))
    )
    early_shares = lax.all_to_all(early_rows, "fs", split_axis=2, concat_axis=1, tiled=True)
    columns_second = join_columns(early_shares[0])
    columns_first = join_columns(early_shares[1])
    columns_cotangent = join_columns(early_shares[2])
    weights_second, columns_second, columns_first, columns_cotangent = lax.optimization_barrier(
        (weights_second, columns_second, columns_first, columns_cotangent)
    )

    partial_second, pieces_second = block_backward(
        norm_second, cotangent, weights_second, width
    )
    all_second = lax.all_gather(pieces_second, "fs", axis=0, tiled=True)
    mid_rows = backward_rows(norm_second, cotangent, gain_second, partial_second)
    mid_grad = join_rows(mid_rows)
    columns_mid = join_columns(share_columns(mid_rows))
    weights_first, pieces_second, mid_grad, columns_mid = lax.optimization_barrier(
        (weights_first, pieces_second, mid_grad, columns_mid)
    )
    partial_first, pieces_first = block_backward(norm_first, mid_grad, weights_first, width)
    all_first = lax.all_gather(pieces_first, "fs", axis=0, tiled=True)
    late_mid = block_forward(late_input, gain_first, weights_first, width)
    input_grad = join_rows(backward_rows(norm_first, mid_grad, gain_first, partial_first))
    late_out = block_forward(late_mid, gain_second, weights_second, width)
    all_second, late_out, input_grad = lax.optimization_barrier((all_second, late_out, input_grad))

    def collect(pieces, columns_in, columns_out, sums):
        return (
            sums[0] + fold_rows(columns_in, pieces[:, :width]),
            sums[1] + fold_rows(columns_in, pieces[:, width : 2 * width]),
            sums[2] + 0.5 * fold_rows(pieces[:, 2 * width :], columns_out),
        )

    new_second = collect(
        all_second, columns_second, columns_cotangent, (sum_gate_second, sum_up_second, sum_down_second)
    )
    all_first, new_second = lax.optimization_barrier((all_first, new_second))
    new_first = collect(
        all_first, columns_first, columns_mid, (sum_gate_first, sum_up_first, sum_down_first)
    )
    return (late_mid, late_out, input_grad) + new_first + new_second


def solution(mesh):
    in_specs = (
        P("fs", None),
        P("fs", None),
        P("fs", None),
        P("fs", None),
        P(),
        P(),
        P("fs", "tp"),
        P("fs", "tp"),
        P("tp", "fs"),
        P("fs", "tp"),
        P("fs", "tp"),
        P("tp", "fs"),
        P("fs", "tp"),
        P("fs", "tp"),
        P("tp", "fs"),
        P("fs", "tp"),
        P("fs", "tp"),
        P("tp", "fs"),
    )
    out_specs = (
        P("fs", None),
        P("fs", None),
        P("fs", None),
        P("fs", "tp"),
        P("fs", "tp"),
        P("tp", "fs"),
        P("fs", "tp"),
        P("fs", "tp"),
        P("tp", "fs"),
    )
    return jax.shard_map(
        per_device, mesh=mesh, in_specs=in_specs, out_specs=out_specs, check_vma=False
    )
```

profile of v0, /device:TPU:0, one launch (start us, length us, event | category | flops | bytes accessed | tf_op | source)
XLA Modules:
  0.0 315.8 jit_solution(12072726947669320214)
XLA Ops:
  7.3 2.4 pad_maximum_fusion.1
  9.8 1.1 pad_maximum_fusion
  11.4 0.9 dynamic-slice_bitcast_fusion.2
  12.3 0.2 multiply_convert_fusion.1
  12.8 0.5 copy-done.4
  13.3 0.2 copy-done.5
  13.6 1.4 copy.83
  14.9 1.6 reshape.147
  16.5 33.2 %all_to_all.70 = bf16[8,2,12288]{2,1,0:T(2,128)(2,1)} all-to-all(bf16[8,2,12288]{2,1,0:T(2,128)(2,1)S(1)} %reshape.147), channel_id=1, replica_groups=mesh['fs'=8,'tp'=4] {'fs'}, dimensions={0} | all-to-all | bytes 786432 | tf_op jit(solution)/shard_map/all_to_all | solution.py:123
  49.8 2.8 reshape.148
  52.6 1.1 copy.105
  53.7 10.2 %all_gather.38 = bf16[1024,256]{1,0:T(8,128)(2,1)S(1)} all-gather(bf16[256,256]{1,0:T(8,128)(2,1)S(1)} %bitcast.67), channel_id=1, replica_groups=mesh['fs'=8,'tp'=4] {'tp'}, dimensions={0}, use_global_device_ids=true | all-gather | bytes 655360 | tf_op jit(solution)/shard_map/all_gather | solution.py:42
  64.0 10.5 %all_gather.39 = bf16[1024,256]{1,0:T(8,128)(2,1)S(1)} all-gather(bf16[256,256]{1,0:T(8,128)(2,1)S(1)} %bitcast.68), channel_id=1, replica_groups=mesh['fs'=8,'tp'=4] {'tp'}, dimensions={0}, use_global_device_ids=true | all-gather | bytes 655360 | tf_op jit(solution)/shard_map/all_gather | solution.py:42
  74.6 9.3 %all_gather.40 = bf16[1024,256]{1,0:T(8,128)(2,1)S(1)} all-gather(bf16[256,256]{1,0:T(8,128)(2,1)S(1)} %bitcast.69), channel_id=1, replica_groups=mesh['fs'=8,'tp'=4] {'tp'}, dimensions={0}, use_global_device_ids=true | all-gather | bytes 655360 | tf_op jit(solution)/shard_map/all_gather | solution.py:42
  83.9 0.8 copy.90
  84.7 22.3 %all-gather.7.cloned.1.call-done = bf16[2048,2112]{0,1:T(8,128)(2,1)} async-done(((bf16[256,2112]{0,1:T(8,128)(2,1)}), bf16[2048,2112]{0,1:T(8,128)(2,1)}) %all-gather.7.cloned.1.call-update) | async-done | bytes 8650768 | tf_op jit(solution)/shard_map/all_gather | solution.py:82
  107.1 4.4 %fusion.10 = f32[128,1408]{0,1:T(8,128)S(1)} fusion(bf16[128,2048]{1,0:T(8,128)(2,1)S(1)} %copy-done.6, bf16[2048,2112]{0,1:T(8,128)(2,1)} %all-gather.7.cloned.1.call-done), kind=kOutput, calls=%fused_computation.10 | convolution fusion | flops 738197504 | bytes 7012352 | tf_op jit(solution)/shard_map/dot_general | solution.py:17
  111.4 2.8 multiply_convert_fusion.11
  114.2 0.8 pad_maximum_fusion.2
  115.1 5.1 %fusion.26 = bf16[128,2048]{1,0:T(8,128)(2,1)} fusion(bf16[2048,2112]{0,1:T(8,128)(2,1)} %all-gather.7.cloned.1.call-done, bf16[128,704]{0,1:T(8,128)(2,1)S(1)} %get-tuple-element.40, bf16[128,704]{0,1:T(8,128)(2,1)S(1)} %get-tuple-element.39), kind=kOutput, calls=%fused_computation.22 | convolution fusion | flops 739180544 | bytes 6651904 | tf_op jit(solution)/shard_map/tf,df->td/dot_general | solution.py:21
  120.2 3.8 %all-to-all-start.1 = ((bf16[4,32,2048]{2,1,0:T(8,128)(2,1)}), bf16[4,32,2048]{2,1,0:T(8,128)(2,1)S(1)}, u32[]{:S(2)}, u32[]{:S(2)}) async-start(bf16[4,32,2048]{2,1,0:T(8,128)(2,1)} %bitcast.20), calls=%async_computation.1 | async-start | bytes 1048576 | tf_op jit(solution)/shard_map/all_to_all | solution.py:34
  124.1 1.1 convert_element_type.92
  125.2 7.3 %all-to-all-done.1 = bf16[4,32,2048]{2,1,0:T(8,128)(2,1)S(1)} async-done(((bf16[4,32,2048]{2,1,0:T(8,128)(2,1)}), bf16[4,32,2048]{2,1,0:T(8,128)(2,1)S(1)}, u32[]{:S(2)}, u32[]{:S(2)}) %all-to-all-start.1) | async-done | bytes 524320 | tf_op jit(solution)/shard_map/all_to_all | solution.py:34
  132.5 1.2 multiply_reduce_fusion.5
  133.7 1.1 add_convert_fusion.3
  134.8 0.7 copy.108
  135.5 3.6 %all-to-all-start.2 = ((bf16[32,8,256]{2,0,1:T(8,128)(2,1)}), bf16[32,8,256]{2,0,1:T(8,128)(2,1)S(1)}, u32[]{:S(2)}, u32[]{:S(2)}) async-start(bf16[32,8,256]{2,0,1:T(8,128)(2,1)} %bitcast.53), calls=%async_computation.2 | async-start | bytes 262144 | tf_op jit(solution)/shard_map/all_to_all | solution.py:86
  139.2 10.6 %all_gather.41 = bf16[128,2048]{1,0:T(8,128)(2,1)S(1)} all-gather(bf16[32,2048]{1,0:T(8,128)(2,1)S(1)} %add_convert_fusion.3), channel_id=1, replica_groups=mesh['fs'=8,'tp'=4] {'tp'}, dimensions={0}, use_global_device_ids=true | all-gather | bytes 655360 | tf_op jit(solution)/shard_map/all_gather | solution.py:42
  149.8 9.3 %all-to-all-done.2 = bf16[32,8,256]{2,0,1:T(8,128)(2,1)S(1)} async-done(((bf16[32,8,256]{2,0,1:T(8,128)(2,1)}), bf16[32,8,256]{2,0,1:T(8,128)(2,1)S(1)}, u32[]{:S(2)}, u32[]{:S(2)}) %all-to-all-start.2) | async-done | bytes 131104 | tf_op jit(solution)/shard_map/all_to_all | solution.py:86
  159.1 10.5 %all_gather.42 = bf16[1024,256]{1,0:T(8,128)(2,1)S(1)} all-gather(bf16[256,256]{1,0:T(8,128)(2,1)S(1)} %bitcast.66), channel_id=1, replica_groups=mesh['fs'=8,'tp'=4] {'tp'}, dimensions={0}, use_global_device_ids=true | all-gather | bytes 655360 | tf_op jit(solution)/shard_map/all_gather | solution.py:42
  169.6 0.8 copy.94
  170.4 25.7 %all-gather.5.cloned.1.call-done = bf16[2048,2112]{0,1:T(8,128)(2,1)} async-done(((bf16[256,2112]{0,1:T(8,128)(2,1)}), bf16[2048,2112]{0,1:T(8,128)(2,1)}) %all-gather.5.cloned.1.call-update) | async-done | bytes 8650768 | tf_op jit(solution)/shard_map/all_gather | solution.py:82
  196.1 4.5 %fusion.2 = f32[128,1408]{0,1:T(8,128)S(1)} fusion(bf16[128,2048]{1,0:T(8,128)(2,1)} %copy-done.4, bf16[2048,2112]{0,1:T(8,128)(2,1)} %all-gather.5.cloned.1.call-done), kind=kOutput, calls=%fused_computation.2 | convolution fusion | flops 738197504 | bytes 7012352 | tf_op jit(solution)/shard_map/dot_general | solution.py:17
  200.6 2.8 multiply_convert_fusion.8
  203.3 0.8 pad_maximum_fusion.3
  204.6 1.0 convert_element_type.90
  205.8 4.7 %fusion.4 = f32[128,1408]{0,1:T(8,128)S(1)} fusion(bf16[2048,2112]{0,1:T(8,128)(2,1)} %all-gather.5.cloned.1.call-done, f32[2048]{0:T(1024)S(1)} %copy-done.17, f32[128]{0:T(128)S(1)} %add_rsqrt_fusion.3, bf16[128,2048]{1,0:T(8,128)(2,1)S(1)} %copy-done.2), kind=kOutput, calls=%fused_computation.4 | convolution fusion | flops 739246080 | bytes 7021056 | tf_op jit(solution)/shard_map/dot_general | solution.py:17
  210.6 3.3 %fusion.23 = bf16[128,2048]{1,0:T(8,128)(2,1)} fusion(bf16[2048,2112]{0,1:T(8,128)(2,1)} %all-gather.5.cloned.1.call-done, f32[128,1408]{0,1:T(8,128)S(1)} %fusion.4), kind=kOutput, calls=%fused_computation.21 | convolution fusion | flops 369901568 | bytes 4128768 | tf_op jit(solution)/shard_map/tf,df->td/dot_general | solution.py:21
  213.8 5.6 %all-to-all-start.3 = ((bf16[4,32,2048]{2,1,0:T(8,128)(2,1)}), bf16[4,32,2048]{2,1,0:T(8,128)(2,1)S(1)}, u32[]{:S(2)}, u32[]{:S(2)}) async-start(bf16[4,32,2048]{2,1,0:T(8,128)(2,1)} %bitcast.26), calls=%async_computation.3 | async-start | bytes 1048576 | tf_op jit(solution)/shard_map/all_to_all | solution.py:34
  219.4 4.5 %fusion.29 = bf16[128,2048]{1,0:T(8,128)(2,1)} fusion(bf16[2048,2112]{0,1:T(8,128)(2,1)} %all-gather.5.cloned.1.call-done, bf16[128,704]{0,1:T(8,128)(2,1)S(1)} %get-tuple-element.38, bf16[128,704]{0,1:T(8,128)(2,1)S(1)} %get-tuple-element.37), kind=kOutput, calls=%fused_computation.23 | convolution fusion | flops 739180544 | bytes 6651904 | tf_op jit(solution)/shard_map/tf,df->td/dot_general | solution.py:21
  223.9 3.9 %all-to-all-done.3 = bf16[4,32,2048]{2,1,0:T(8,128)(2,1)S(1)} async-done(((bf16[4,32,2048]{2,1,0:T(8,128)(2,1)}), bf16[4,32,2048]{2,1,0:T(8,128)(2,1)S(1)}, u32[]{:S(2)}, u32[]{:S(2)}) %all-to-all-start.3) | async-done | bytes 524320 | tf_op jit(solution)/shard_map/all_to_all | solution.py:34
  227.8 3.5 %all-to-all-start.5 = ((bf16[4,32,2048]{2,1,0:T(8,128)(2,1)}), bf16[4,32,2048]{2,1,0:T(8,128)(2,1)S(1)}, u32[]{:S(2)}, u32[]{:S(2)}) async-start(bf16[4,32,2048]{2,1,0:T(8,128)(2,1)} %bitcast.72), calls=%async_computation.5 | async-start | bytes 1048576 | tf_op jit(solution)/shard_map/all_to_all | solution.py:34
  231.4 1.0 add_convert_fusion.2
  232.4 12.4 %all_gather.43 = bf16[128,2048]{1,0:T(8,128)(2,1)S(1)} all-gather(bf16[32,2048]{1,0:T(8,128)(2,1)S(1)} %add_convert_fusion.2), channel_id=1, replica_groups=mesh['fs'=8,'tp'=4] {'tp'}, dimensions={0}, use_global_device_ids=true | all-gather | bytes 655360 | tf_op jit(solution)/shard_map/all_gather | solution.py:42
  245.0 4.4 %fusion.6 = f32[128,1408]{0,1:T(8,128)S(1)} fusion(bf16[2048,2112]{0,1:T(8,128)(2,1)} %all-gather.7.cloned.1.call-done, f32[128]{0:T(128)S(1)} %add_rsqrt_fusion, bf16[128,2048]{1,0:T(8,128)(2,1)S(1)} %all_gather.43, f32[2048]{0:T(1024)S(1)} %copy-done.16), kind=kOutput, calls=%fused_computation.6 | convolution fusion | flops 739246080 | bytes 7021056 | tf_op jit(solution)/shard_map/dot_general | solution.py:17
  249.4 1.1 convert_element_type.107
  250.5 3.3 %fusion.20 = bf16[128,2048]{1,0:T(8,128)(2,1)} fusion(bf16[2048,2112]{0,1:T(8,128)(2,1)} %all-gather.7.cloned.1.call-done, f32[128,1408]{0,1:T(8,128)S(1)} %fusion.6), kind=kOutput, calls=%fused_computation.20 | convolution fusion | flops 369901568 | bytes 4128768 | tf_op jit(solution)/shard_map/tf,df->td/dot_general | solution.py:21
  253.8 4.2 %all-to-all-start.4 = ((bf16[4,32,2048]{2,1,0:T(8,128)(2,1)}), bf16[4,32,2048]{2,1,0:T(8,128)(2,1)}, u32[]{:S(2)}, u32[]{:S(2)}) async-start(bf16[4,32,2048]{2,1,0:T(8,128)(2,1)} %bitcast.73), calls=%async_computation.4 | async-start | bytes 1048576 | tf_op jit(solution)/shard_map/all_to_all | solution.py:34
  258.1 0.2 multiply_reduce_fusion.4
  258.3 1.0 add_convert_fusion
  259.3 11.1 %all_gather.46 = bf16[128,2048]{1,0:T(8,128)(2,1)S(1)} all-gather(bf16[32,2048]{1,0:T(8,128)(2,1)S(1)} %add_convert_fusion), channel_id=1, replica_groups=mesh['fs'=8,'tp'=4] {'tp'}, dimensions={0}, use_global_device_ids=true | all-gather | bytes 655360 | tf_op jit(solution)/shard_map/all_gather | solution.py:42
  270.4 1.1 convert_reduce_fusion.1
  271.5 1.0 add_convert_fusion.1
  272.5 10.8 %all_gather.45 = bf16[128,2048]{1,0:T(8,128)(2,1)S(1)} all-gather(bf16[32,2048]{1,0:T(8,128)(2,1)S(1)} %add_convert_fusion.1), channel_id=1, replica_groups=mesh['fs'=8,'tp'=4] {'tp'}, dimensions={0}, use_global_device_ids=true | all-gather | bytes 655360 | tf_op jit(solution)/shard_map/all_gather | solution.py:42
  283.4 2.9 fusion.47
  286.3 2.8 fusion.44
  289.2 2.8 fusion.53
  292.0 6.4 %all-gather.11.cloned.1.call-done = bf16[1024,2112]{0,1:T(8,128)(2,1)} async-done(((bf16[128,2112]{0,1:T(8,128)(2,1)}), bf16[1024,2112]{0,1:T(8,128)(2,1)}) %all-gather.11.cloned.1.call-update) | async-done | bytes 4325392 | tf_op jit(solution)/shard_map/all_gather | solution.py:142
  298.3 2.8 fusion.59
  301.2 2.9 fusion.56
  304.1 2.8 fusion.65
  306.9 0.8 copy.112
  307.7 0.8 copy.113
  308.5 0.8 copy.114
  (82 shorter events, 2.2 us)
Async XLA Ops:
  7.2 2.6 copy-start.12
  7.2 2.6 copy-start.14
  7.2 2.6 copy-start.13
  7.2 99.9 %all-gather.7.cloned.1.call-start = ((), (), s32[]{:S(2)}) async-start(), calls=%async_computation.7 | async-start | bytes 9732096 | tf_op jit(solution)/shard_map/all_gather | solution.py:82
  7.3 3.7 %copy-start.1 = (bf16[128,2048]{1,0:T(8,128)(2,1)S(1)}, bf16[128,2048]{1,0:T(8,128)(2,1)}, u32[]{:S(2)}) copy-start(bf16[128,2048]{1,0:T(8,128)(2,1)} %param.19) | copy-start | bytes 1572868
  9.6 1.5 copy-start
  9.6 2.6 copy-start.17
  9.7 2.8 copy-start.16
  9.7 186.4 %all-gather.5.cloned.1.call-start = ((), (), s32[]{:S(2)}) async-start(), calls=%async_computation.6 | async-start | bytes 9732096 | tf_op jit(solution)/shard_map/all_gather | solution.py:82
  10.9 272.5 %all-gather.9.cloned.1.call-start = ((), (), s32[]{:S(2)}) async-start(), calls=%async_computation.8 | async-start | bytes 4866048 | tf_op jit(solution)/shard_map/all_gather | solution.py:134
  11.3 1.4 copy-start.18
  11.3 1.4 copy-start.20
  12.5 0.8 copy-start.4
  12.7 0.8 copy-start.5
  53.7 53.3 %copy-start.6 = (bf16[128,2048]{1,0:T(8,128)(2,1)S(1)}, bf16[128,2048]{1,0:T(8,128)(2,1)}, u32[]{:S(2)}) copy-start(bf16[128,2048]{1,0:T(8,128)(2,1)} %copy-done.5) | copy-start | bytes 1572868
  107.1 4.4 %copy-start.15 = (bf16[128,2048]{1,0:T(8,128)(2,1)S(1)}, bf16[128,2048]{1,0:T(8,128)(2,1)}, u32[]{:S(2)}) copy-start(bf16[128,2048]{1,0:T(8,128)(2,1)} %param.21) | copy-start | bytes 1572868
  115.1 8.9 %copy-start.21 = (f32[128]{0:T(128)S(1)}, f32[128]{0:T(128)}, u32[]{:S(2)}) copy-start(f32[128]{0:T(128)} %copy-done.20) | copy-start | bytes 1540
  120.2 12.3 %all-to-all-start.1 = ((bf16[4,32,2048]{2,1,0:T(8,128)(2,1)}), bf16[4,32,2048]{2,1,0:T(8,128)(2,1)S(1)}, u32[]{:S(2)}, u32[]{:S(2)}) async-start(bf16[4,32,2048]{2,1,0:T(8,128)(2,1)} %bitcast.20), calls=%async_computation.1 | async-start | bytes 1048576 | tf_op jit(solution)/shard_map/all_to_all | solution.py:34
  135.5 23.6 %all-to-all-start.2 = ((bf16[32,8,256]{2,0,1:T(8,128)(2,1)}), bf16[32,8,256]{2,0,1:T(8,128)(2,1)S(1)}, u32[]{:S(2)}, u32[]{:S(2)}) async-start(bf16[32,8,256]{2,0,1:T(8,128)(2,1)} %bitcast.53), calls=%async_computation.2 | async-start | bytes 262144 | tf_op jit(solution)/shard_map/all_to_all | solution.py:86
  139.1 159.2 %all-gather.11.cloned.1.call-start = ((), (), s32[]{:S(2)}) async-start(), calls=%async_computation.9 | async-start | bytes 4866048 | tf_op jit(solution)/shard_map/all_gather | solution.py:142
  149.8 50.7 %copy-start.3 = (bf16[128,2048]{1,0:T(8,128)(2,1)}, bf16[128,2048]{1,0:T(8,128)(2,1)S(1)}, u32[]{:S(2)}) copy-start(bf16[128,2048]{1,0:T(8,128)(2,1)S(1)} %all_gather.41) | copy-start | bytes 1572868
  200.5 3.6 %copy-start.19 = (f32[128]{0:T(128)S(1)}, f32[128]{0:T(128)}, u32[]{:S(2)}) copy-start(f32[128]{0:T(128)} %copy-done.18) | copy-start | bytes 1540
  203.3 1.2 copy-start.2
  213.8 14.0 %all-to-all-start.3 = ((bf16[4,32,2048]{2,1,0:T(8,128)(2,1)}), bf16[4,32,2048]{2,1,0:T(8,128)(2,1)S(1)}, u32[]{:S(2)}, u32[]{:S(2)}) async-start(bf16[4,32,2048]{2,1,0:T(8,128)(2,1)} %bitcast.26), calls=%async_computation.3 | async-start | bytes 1048576 | tf_op jit(solution)/shard_map/all_to_all | solution.py:34
  227.8 26.0 %all-to-all-start.5 = ((bf16[4,32,2048]{2,1,0:T(8,128)(2,1)}), bf16[4,32,2048]{2,1,0:T(8,128)(2,1)S(1)}, u32[]{:S(2)}, u32[]{:S(2)}) async-start(bf16[4,32,2048]{2,1,0:T(8,128)(2,1)} %bitcast.72), calls=%async_computation.5 | async-start | bytes 1048576 | tf_op jit(solution)/shard_map/all_to_all | solution.py:34
  253.8 16.6 %all-to-all-start.4 = ((bf16[4,32,2048]{2,1,0:T(8,128)(2,1)}), bf16[4,32,2048]{2,1,0:T(8,128)(2,1)}, u32[]{:S(2)}, u32[]{:S(2)}) async-start(bf16[4,32,2048]{2,1,0:T(8,128)(2,1)} %bitcast.73), calls=%async_computation.4 | async-start | bytes 1048576 | tf_op jit(solution)/shard_map/all_to_all | solution.py:34
  258.1 25.3 %copy-start.7 = (f32[256,704]{0,1:T(8,128)S(1)}, f32[256,704]{0,1:T(8,128)}, u32[]{:S(2)}) copy-start(f32[256,704]{0,1:T(8,128)} %param.34) | copy-start | bytes 2162692
  283.4 2.9 copy-start.8
  283.4 5.8 %copy-start.10 = (bf16[4,8,32,256]{3,2,0,1:T(8,128)(2,1)S(1)}, bf16[4,8,32,256]{3,2,0,1:T(8,128)(2,1)}, u32[]{:S(2)}) copy-start(bf16[4,8,32,256]{3,2,0,1:T(8,128)(2,1)} %copy.90) | copy-start | bytes 1572868
  283.4 5.8 %copy-start.22 = (f32[704,256]{1,0:T(8,128)S(1)}, f32[704,256]{1,0:T(8,128)}, u32[]{:S(2)}) copy-start(f32[704,256]{1,0:T(8,128)} %param.35) | copy-start | bytes 2162692
  286.3 12.0 %copy-start.9 = (f32[256,704]{0,1:T(8,128)S(1)}, f32[256,704]{0,1:T(8,128)}, u32[]{:S(2)}) copy-start(f32[256,704]{0,1:T(8,128)} %param.31) | copy-start | bytes 2162692
  292.0 12.2 %copy-start.11 = (bf16[4,8,32,256]{3,2,0,1:T(8,128)(2,1)S(1)}, bf16[4,8,32,256]{3,2,0,1:T(8,128)(2,1)}, u32[]{:S(2)}) copy-start(bf16[4,8,32,256]{3,2,0,1:T(8,128)(2,1)} %copy.94) | copy-start | bytes 1572868
  298.3 5.8 %copy-start.23 = (f32[704,256]{1,0:T(8,128)S(1)}, f32[704,256]{1,0:T(8,128)}, u32[]{:S(2)}) copy-start(f32[704,256]{1,0:T(8,128)} %param.32) | copy-start | bytes 2162692
Sparse Core Ops, SparseCore 0:
  9.8 97.2 all-gather.6
  108.6 87.3 all-gather.4
  198.2 50.9 all-gather.8
  251.2 47.0 all-gather.10
where the time goes:
time: 317 us; the launch traced here: 316 us
  blocking collectives  119 us (38%)
  waiting for transfers between devices  74.9 us (24%)
  matrix products  56.6 us (18%)
  starting transfers between devices  20.8 us (7%)
  other arithmetic  16.6 us (5%)
  between operations  14.2 us (4%)
  local copies, waits for them, and re-layouts  13.9 us (4%)
    all_gather x8, blocking collectives, join_rows(): return lax.all_gather(rows, 'tp', axis=0, tiled=True)  85.4 us
    all_gather x2, waiting for transfers between devices, gather_weights(): lax.all_gather(jnp.concatenate((gate, up, down.T), axis=1), 'fs', axis=0,...  48 us
    all_to_all x1, blocking collectives, per_device(): lax.all_to_all(early_rows, 'fs', split_axis=2, concat_axis=1, tiled=True)  33.2 us
    dot_general x6, matrix products, project(): return jnp.dot(rows, weights, preferred_element_type=jnp.float32)  23.5 us
    dot_general x6, matrix products, fold_rows(): jnp.einsum('ta,tb->ab', left, right, preferred_element_type=jnp.float32)  17 us
    all_to_all x4, starting transfers between devices, sum_rows(): lax.all_to_all(partial.astype(jnp.bfloat16), 'tp', split_axis=0, concat_a...  17 us
    dot_general x4, matrix products, project_back(): jnp.einsum('tf,df->td', hidden_rows, weights, preferred_element_type=jnp....  16.1 us
    all_to_all x4, waiting for transfers between devices, sum_rows(): lax.all_to_all(partial.astype(jnp.bfloat16), 'tp', split_axis=0, concat_a...  11.2 us
  transfers between devices with their start and end apart: 9, of which 6 were waited for; matrix products, arithmetic and copies ran while one was open for 23% of the time, Pallas kernels for 0%

commit v1 on v0

--- a/solution.py
+++ b/solution.py
@@ -1,9 +1,627 @@
+import functools
+
 import jax
 import jax.numpy as jnp
 from jax import lax
+from jax.experimental import pallas as pl
+from jax.experimental.pallas import tpu as pltpu
 from jax.sharding import PartitionSpec as P
 
 norm_eps = 1e-06
+CORES = 2
+TP = 4
+PLANES = 4
+
+NT = (((1,), (1,)), ((), ()))
+NN = (((1,), (0,)), ((), ()))
+TN = (((0,), (0,)), ((), ()))
+
+
+def mm(left, right, dims):
+    return lax.dot_general(left, right, dims, preferred_element_type=jnp.float32)
+
+
+def norm_parts(rows):
+    wide = rows.astype(jnp.float32)
+    factor = lax.rsqrt(jnp.mean(wide * wide, axis=-1, keepdims=True) + norm_eps)
+    return wide, factor
+
+
+def step_kernel(
+    late_in, mid_in, cot_in, early_in, gain2, gain1, w2, w1,
+    out_rows, g20, g21, g22, g10, g11, g12,
+    weights, acts, late, normed, late_normed, pieces, pieces_in, cols_in,
+    part, part_in2, part_in1, late_part, late_part_in, sent, back_rows, done_rows,
+    acc, late_acc, late_hid, send_sems, recv_sems, local_sems, ack,
+):
+    f, t = lax.axis_index("fs"), lax.axis_index("tp")
+    z, core = f // CORES, f % CORES
+    peer = 1 - core
+    inner = (z == 1) | (z == 2)
+    outer = (z == 0) | (z == 3)
+    near, upper = (z // 2) * 3, z // 2
+    q = late_in.shape[0] // TP
+    rows = PLANES * q
+    half = 2 * q
+    width = w2.shape[1]
+    hidden = w2.shape[0] // 3
+    tile = TP * half
+    grads = ((g20, g21, g22), (g10, g11, g12))
+    shards = (w2, w1)
+    gains = (gain2, gain1)
+    ids = {}
+
+    def sem(name):
+        return ids.setdefault(name, len(ids))
+
+    def column(mask):
+        x, y = t % 2, t // 2
+        gx, gy = mask % 2, mask // 2
+        x = x + gx - 2 * x * gx
+        y = y + gy - 2 * y * gy
+        return y * 2 + x
+
+    def device(zz, cc, tt):
+        return (zz * CORES + cc, tt)
+
+    def remote(src, dst, index, where):
+        return pltpu.make_async_remote_copy(
+            src_ref=src, dst_ref=dst, send_sem=send_sems.at[index],
+            recv_sem=recv_sems.at[index], device_id=where,
+            device_id_type=pl.DeviceIdType.MESH,
+        )
+
+    def local(src, dst, index):
+        return pltpu.make_async_copy(src, dst, local_sems.at[index])
+
+    def own_quarter(tt):
+        return pl.ds(pl.multiple_of(tt * q, q), q)
+
+    def feature(slot, other):
+        v = slot + (1 - slot // 2) * (1 - 2 * slot)
+        zs = v + upper * (3 - 2 * v)
+        cc = core + other - 2 * core * other
+        return pl.ds(pl.multiple_of((zs * CORES + cc) * width, width), width)
+
+    barrier = pltpu.get_barrier_semaphore()
+    friends = [device((z + k) % PLANES, core, t) for k in range(1, PLANES)]
+    friends += [device(z, peer, t)] + [device(z, core, column(m)) for m in range(1, TP)]
+    for friend in friends:
+        pl.semaphore_signal(barrier, inc=1, device_id=friend, device_id_type=pl.DeviceIdType.MESH)
+    pl.semaphore_wait(barrier, len(friends))
+
+    mine = own_quarter(t)
+    z_items = []
+    for name, src, to in (
+        ("m", mid_in, lambda s: acts.at[0, 0, pl.ds(s * q, q)]),
+        ("c", cot_in, lambda s: acts.at[1, 0, pl.ds(s * q, q)]),
+    ):
+        z_items.append((name, src.at[mine], to))
+    z_items.append(("w0", w2, lambda s: weights.at[0, s]))
+    z_items.append(("e", early_in.at[mine], lambda s: acts.at[2, 0, pl.ds(s * q, q)]))
+    z_items.append(("l", late_in.at[mine], lambda s: late.at[0, 0, pl.ds(s * q, q)]))
+    z_items.append(("w1", w1, lambda s: weights.at[1, s]))
+    z_base = {}
+    for name, _, _ in z_items:
+        z_base[name] = sem((name, 0))
+        for s in range(1, 4):
+            sem((name, s))
+
+    def z_copy(item, s, where):
+        name, src, to = item
+        return remote(src, to(s), z_base[name] + s, where)
+
+    first_target = device(1 + upper, core, t)
+    second_target = device(2 - upper, core, t)
+    mid_target = device(3 - z, core, t)
+
+    def outer_sends():
+        out = []
+        for item in z_items:
+            out.append(z_copy(item, 1, first_target))
+            if item[0] != "l":
+                out.append(z_copy(item, 3, second_target))
+        return out
+
+    def inner_sends():
+        return [z_copy(item, 2, mid_target) for item in z_items if item[0] != "l"]
+
+    out_dev = device(near, core, t)
+
+    def grad_back(b, j):
+        return remote(sent[3 * b + j], grads[b][j], sem(("g", b, j)), out_dev)
+
+    def row_source(k):
+        return (late.at[1, 0], done_rows.at[0], done_rows.at[1])[k]
+
+    def rows_back(k):
+        return remote(row_source(k).at[pl.ds(q, q)], back_rows.at[k], sem(("r", k)), out_dev)
+
+    def deliver(k, m, src):
+        return remote(src, out_rows.at[k, mine], sem(("d", k, m)), device(z, core, column(m)))
+
+    def deliver_wait(k, m):
+        other = column(m)
+        dst = out_rows.at[k, own_quarter(other)]
+        remote(dst, dst, sem(("d", k, m)), device(z, core, other)).wait_recv()
+
+    for b in range(2):
+        for j in range(3):
+            sem(("g", b, j))
+    for k in range(3):
+        sem(("r", k))
+        for m in range(1, TP):
+            sem(("d", k, m))
+
+    @pl.when(outer)
+    def _():
+        for copy in outer_sends():
+            copy.start()
+        for k in (0, 1, 2):
+            rows_back(k).wait_recv()
+            for m in range(1, TP):
+                deliver(k, m, back_rows.at[k]).start()
+            out_rows[k, mine, :] = back_rows[k]
+        for copy in outer_sends():
+            copy.wait_send()
+        for b in range(2):
+            for j in range(3):
+                grad_back(b, j).wait_recv()
+        for k in range(3):
+            for m in range(1, TP):
+                deliver(k, m, back_rows.at[k]).wait_send()
+                deliver_wait(k, m)
+
+    @pl.when(inner)
+    def _():
+        for copy in inner_sends():
+            copy.start()
+        peer_dev = device(z, peer, t)
+
+        def shard_local(b):
+            return local(shards[b], weights.at[b, 0], b)
+
+        w_base = []
+        for b in range(2):
+            w_base.append(sem(("p", b, 0)))
+            for s in range(1, 4):
+                sem(("p", b, s))
+
+        def shard_forward(b, s, src):
+            return remote(src, weights.at[b, 4 + s], w_base[b] + s, peer_dev)
+
+        def row_locals(a):
+            src = (mid_in, cot_in, early_in, late_in)[a]
+            out = []
+            for m in range(TP):
+                dst = late.at[0, m, pl.ds(0, q)] if a == 3 else acts.at[a, m, pl.ds(0, q)]
+                out.append(local(src.at[own_quarter(column(m))], dst, 2 + TP * a + m))
+            return out
+
+        for b in range(2):
+            shard_local(b).start()
+            shard_forward(b, 0, shards[b]).start()
+        for a in range(4):
+            for copy in row_locals(a):
+                copy.start()
+
+        def spread_rows(a):
+            src = (acts.at[a, 0], late.at[0, 0])[a == 3].at[pl.ds(q, q if a == 3 else 3 * q)]
+            out = []
+            for m in range(1, TP):
+                full = late.at[0, m] if a == 3 else acts.at[a, m]
+                dst = full.at[pl.ds(q, q if a == 3 else 3 * q)]
+                out.append(remote(src, dst, sem(("s", a, m)), device(z, core, column(m))))
+            return out
+
+        def z_arrived(index, s):
+            item = z_items[index]
+            remote(item[2](s), item[2](s), z_base[item[0]] + s, mid_target).wait_recv()
+
+        def gather_rows(a, index):
+            for s in (1,) if a == 3 else (1, 2, 3):
+                z_arrived(index, s)
+            for copy in spread_rows(a):
+                copy.start()
+
+        def rows_ready(a):
+            for copy in row_locals(a):
+                copy.wait()
+            for copy in spread_rows(a):
+                copy.wait_recv()
+
+        gather_rows(0, 0)
+        gather_rows(1, 1)
+
+        def normalize_block(b):
+            @pl.loop(0, TP * PLANES)
+            def _(i):
+                at = pl.ds(pl.multiple_of((i % PLANES) * q, q), q)
+                wide, factor = norm_parts(acts[2 * b, i // PLANES, at, :])
+                normed[i // PLANES, at, :] = (wide * factor * gains[b][...]).astype(jnp.bfloat16)
+
+        def rows_of(ref, h, cols):
+            at = pl.ds(pl.multiple_of(h * half, half), half)
+            return ref[:, at, cols].reshape(tile, width)
+
+        def pre_block(b):
+            acc[...] = jnp.zeros_like(acc)
+
+            @pl.loop(0, 8)
+            def _(i):
+                slot, other = i // 2, i % 2
+
+                @pl.when(i == 0)
+                def _():
+                    shard_local(b).wait()
+
+                @pl.when((i > 0) & (other == 0))
+                def _():
+                    ref = weights.at[b, slot]
+                    remote(ref, ref, z_base["w%d" % b] + slot, mid_target).wait_recv()
+                    shard_forward(b, slot, ref).start()
+
+                @pl.when(other == 1)
+                def _():
+                    ref = weights.at[b, 4 + slot]
+                    remote(ref, ref, w_base[b] + slot, peer_dev).wait_recv()
+
+                at = slot + 4 * other
+                cols = feature(slot, other)
+
+                @pl.loop(0, 2)
+                def _(h):
+                    piece = rows_of(normed, h, cols)
+                    for j in range(2):
+                        w = weights[b, at, pl.ds(j * hidden, hidden), :]
+                        acc[j, h] += mm(piece, w, NT)
+
+        def pieces_block(b):
+            cots = acts.at[2 * b + 1]
+
+            @pl.loop(0, 2)
+            def _(h):
+                late_acc[0] = jnp.zeros_like(late_acc[0])
+
+                @pl.loop(0, 8)
+                def _(i):
+                    cols = feature(i % 4, i // 4)
+                    w = weights[b, i, pl.ds(2 * hidden, hidden), :]
+                    late_acc[0] += mm(rows_of(cots, h, cols), w, NT)
+
+                @pl.loop(0, TP)
+                def _(m):
+                    at = pl.ds(pl.multiple_of(m * half, half), half)
+                    to = pl.ds(pl.multiple_of(h * half, half), half)
+                    gate, up = acc[0, h, at, :], acc[1, h, at, :]
+                    grad = 0.5 * late_acc[0, at, :]
+                    sig = 1.0 / (1.0 + jnp.exp(-gate))
+                    act = gate * sig
+                    turn = sig * (1.0 + gate * (1.0 - sig))
+                    pieces[0, m, to, :] = (grad * up * turn).astype(jnp.bfloat16)
+                    pieces[1, m, to, :] = (grad * act).astype(jnp.bfloat16)
+                    pieces[2, m, to, :] = (act * up).astype(jnp.bfloat16)
+
+        def swaps(b):
+            out = []
+            for j in range(3):
+                out.append(remote(pieces.at[j], pieces_in.at[j], sem(("x", b, j)), peer_dev))
+            for k in range(2):
+                cols = feature(k, 1)
+                for j, src in enumerate((normed, acts.at[2 * b + 1])):
+                    out.append(
+                        remote(src.at[:, :, cols], cols_in.at[j, k], sem(("y", b, j, k)), peer_dev)
+                    )
+            return out
+
+        def part_copy(b, h, m, base):
+            at = pl.ds(pl.multiple_of(h * half, half), half)
+            dst = (part_in2, part_in1)[b]
+            return remote(
+                part.at[m, at], dst.at[m - 1, at], base + h * 3 + (m - 1),
+                device(z, core, column(m)),
+            )
+
+        part_base = []
+        for b in range(2):
+            part_base.append(sem(("n", b, 0)))
+            for i in range(1, 6):
+                sem(("n", b, i))
+
+        def grad_part(b):
+            @pl.loop(0, 2 - b)
+            def _(h):
+                at = pl.ds(pl.multiple_of(h * half, half), half)
+
+                @pl.loop(0, 8)
+                def _(i):
+                    cols = feature(i % 4, i // 4)
+                    total = None
+                    for j in range(2):
+                        left = pieces[j, :, at, :].reshape(tile, hidden)
+                        w = weights[b, i, pl.ds(j * hidden, hidden), :]
+                        one = mm(left, w, NN)
+                        total = one if j == 0 else total + one
+                    part[:, at, cols] = total.astype(jnp.bfloat16).reshape(TP, half, width)
+
+                for m in range(1, TP):
+                    part_copy(b, h, m, part_base[b]).start()
+
+        def fold(b):
+            for copy in swaps(b):
+                copy.wait_recv()
+            tokens = TP * rows
+            cots = acts.at[2 * b + 1]
+            for k in range(2):
+                cols = feature(k, 0)
+                outs = grads[b] if k == 0 else sent[3 * b : 3 * b + 3]
+                a0 = normed[:, :, cols].reshape(tokens, width)
+                a1 = cols_in[0, k].reshape(tokens, width)
+                for j in range(2):
+                    one = mm(a0, pieces[j].reshape(tokens, hidden), TN)
+                    one = one + mm(a1, pieces_in[j].reshape(tokens, hidden), TN)
+                    outs[j][...] = one.astype(jnp.bfloat16)
+                one = mm(pieces[2].reshape(tokens, hidden), cots[:, :, cols].reshape(tokens, width), TN)
+                one = one + mm(
+                    pieces_in[2].reshape(tokens, hidden), cols_in[1, k].reshape(tokens, width), TN
+                )
+                outs[2][...] = (0.5 * one).astype(jnp.bfloat16)
+            for j in range(3):
+                grad_back(b, j).start()
+
+        def rows_grad(b, h, store):
+            arrived = (part_in2, part_in1)[b]
+
+            @pl.loop(0, 2)
+            def _(i):
+                at = pl.ds(pl.multiple_of(h * half + i * q, q), q)
+                total = part[0, at, :].astype(jnp.float32)
+                for m in range(1, TP):
+                    total = total + arrived[m - 1, at, :].astype(jnp.float32)
+                wide, factor = norm_parts(acts[2 * b, 0, at, :])
+                scaled = total * gains[b][...]
+                unit = wide * factor
+                inner_mean = jnp.mean(scaled * unit, axis=-1, keepdims=True)
+                cot = acts[2 * b + 1, 0, at, :].astype(jnp.float32)
+                store(at, (cot + factor * (scaled - unit * inner_mean)).astype(jnp.bfloat16))
+
+        def mid_copy(h, m, base):
+            at = pl.ds(pl.multiple_of(h * half, half), half)
+            return remote(
+                acts.at[3, 0, at], acts.at[3, m, at], base + h * 3 + (m - 1),
+                device(z, core, column(m)),
+            )
+
+        mid_base = sem(("a", 0))
+        for i in range(1, 6):
+            sem(("a", i))
+
+        def late_block(b, n):
+            @pl.loop(0, TP * 2)
+            def _(i):
+                at = pl.ds(pl.multiple_of((i % 2) * q, q), q)
+                wide, factor = norm_parts(late[n, i // 2, at, :])
+                late_normed[i // 2, at, :] = (wide * factor * gains[b][...]).astype(jnp.bfloat16)
+
+            late_acc[...] = jnp.zeros_like(late_acc)
+
+            @pl.loop(0, 8)
+            def _(i):
+                cols = feature(i % 4, i // 4)
+                piece = late_normed[:, :, cols].reshape(tile, width)
+                for j in range(2):
+                    w = weights[b, i, pl.ds(j * hidden, hidden), :]
+                    late_acc[j] += mm(piece, w, NT)
+
+            gate = late_acc[0]
+            hid = (gate / (1.0 + jnp.exp(-gate)) * late_acc[1]).astype(jnp.bfloat16)
+            late_hid[...] = hid
+
+            @pl.loop(0, 8)
+            def _(i):
+                cols = feature(i % 4, i // 4)
+                w = weights[b, i, pl.ds(2 * hidden, hidden), :]
+                one = mm(late_hid[...], w, NN).astype(jnp.bfloat16)
+                late_part[:, :, cols] = one.reshape(TP, half, width)
+
+            for m in range(1, TP):
+                late_copy(n, m).start()
+
+        def late_copy(n, m):
+            return remote(
+                late_part.at[m], late_part_in.at[n, m - 1], sem(("h", n, m)),
+                device(z, core, column(m)),
+            )
+
+        def late_sum(n, store):
+            for m in range(1, TP):
+                late_copy(n, m).wait_recv()
+
+            @pl.loop(0, 2)
+            def _(i):
+                at = pl.ds(pl.multiple_of(i * q, q), q)
+                total = late_part[0, at, :].astype(jnp.float32)
+                for m in range(1, TP):
+                    total = total + late_part_in[n, m - 1, at, :].astype(jnp.float32)
+                value = late[n, 0, at, :].astype(jnp.float32) + 0.5 * total
+                store(at, value.astype(jnp.bfloat16))
+
+        def late_spread(m):
+            return remote(
+                late.at[1, 0], late.at[1, m], sem(("k", m)), device(z, core, column(m))
+            )
+
+        rows_ready(0)
+        normalize_block(0)
+        pre_block(0)
+        rows_ready(1)
+        pieces_block(0)
+        for copy in swaps(0):
+            copy.start()
+        grad_part(0)
+        gather_rows(2, 3)
+        gather_rows(3, 4)
+        fold(0)
+
+        def keep_mid(at, value):
+            acts[3, 0, at, :] = value
+
+        for h in range(2):
+            for m in range(1, TP):
+                part_copy(0, h, m, part_base[0]).wait_recv()
+            rows_grad(0, h, keep_mid)
+            for m in range(1, TP):
+                mid_copy(h, m, mid_base).start()
+        for copy in swaps(0):
+            copy.wait_send()
+        pl.semaphore_signal(ack, inc=1, device_id=peer_dev, device_id_type=pl.DeviceIdType.MESH)
+
+        rows_ready(2)
+        normalize_block(1)
+        pre_block(1)
+        rows_ready(3)
+        late_block(1, 0)
+        for h in range(2):
+            for m in range(1, TP):
+                mid_copy(h, m, mid_base).wait_recv()
+        pieces_block(1)
+        pl.semaphore_wait(ack, 1)
+        for copy in swaps(1):
+            copy.start()
+        for h in range(2):
+            for m in range(1, TP):
+                part_copy(0, h, m, part_base[0]).wait_send()
+        grad_part(1)
+
+        def keep_late(at, value):
+            late[1, 0, at, :] = value
+
+        late_sum(0, keep_late)
+        for m in range(1, TP):
+            late_spread(m).start()
+        rows_back(0).start()
+        fold(1)
+        for m in range(1, TP):
+            late_spread(m).wait_recv()
+            late_copy(0, m).wait_send()
+        late_block(0, 1)
+        for m in range(1, TP):
+            part_copy(1, 0, m, part_base[1]).wait_recv()
+
+        def keep_done(index):
+            def store(at, value):
+                done_rows[index, at, :] = value
+
+            return store
+
+        rows_grad(1, 0, keep_done(1))
+        rows_back(2).start()
+        late_sum(1, keep_done(0))
+        rows_back(1).start()
+        for k in range(3):
+            src = row_source(k).at[pl.ds(0, q)]
+            for m in range(1, TP):
+                deliver(k, m, src).start()
+            out_rows[k, mine, :] = src[...]
+
+        for copy in inner_sends():
+            copy.wait_send()
+        for b in range(2):
+            for s in range(4):
+                src = shards[b] if s == 0 else weights.at[b, s]
+                shard_forward(b, s, src).wait_send()
+            for j in range(3):
+                grad_back(b, j).wait_send()
+        for a in range(4):
+            for copy in spread_rows(a):
+                copy.wait_send()
+        for copy in swaps(1):
+            copy.wait_send()
+        for m in range(1, TP):
+            for h in range(2):
+                mid_copy(h, m, mid_base).wait_send()
+            part_copy(1, 0, m, part_base[1]).wait_send()
+            late_spread(m).wait_send()
+            late_copy(1, m).wait_send()
+        for k in range(3):
+            rows_back(k).wait_send()
+            for m in range(1, TP):
+                deliver(k, m, row_source(k).at[pl.ds(0, q)]).wait_send()
+                deliver_wait(k, m)
+
+
+def per_device(
+    late_input,
+    early_input,
+    early_mid,
+    cotangent,
+    gain_first,
+    gain_second,
+    gate_first,
+    up_first,
+    down_first,
+    gate_second,
+    up_second,
+    down_second,
+    *sums,
+):
+    count, feats = late_input.shape
+    width, hidden = gate_first.shape
+    q = count // TP
+    half = 2 * q
+    tile = TP * half
+    bf = jnp.bfloat16
+    shard_second = jnp.concatenate((gate_second.T, up_second.T, down_second), axis=0)
+    shard_first = jnp.concatenate((gate_first.T, up_first.T, down_first), axis=0)
+    wide, tall = (width, hidden), (hidden, width)
+    grad_shapes = [wide, wide, tall] * 2
+    anywhere = pl.BlockSpec(memory_space=pl.ANY)
+    in_vmem = pl.BlockSpec(memory_space=pltpu.VMEM)
+    outs = pl.pallas_call(
+        step_kernel,
+        out_shape=[jax.ShapeDtypeStruct((3, count, feats), bf)]
+        + [jax.ShapeDtypeStruct(s, bf) for s in grad_shapes],
+        in_specs=[anywhere] * 4 + [in_vmem] * 2 + [anywhere] * 2,
+        out_specs=[in_vmem] * 7,
+        scratch_shapes=[
+            pltpu.VMEM((2, 8, 3 * hidden, width), bf),
+            pltpu.VMEM((4, TP, count, feats), bf),
+            pltpu.VMEM((2, TP, half, feats), bf),
+            pltpu.VMEM((TP, count, feats), bf),
+            pltpu.VMEM((TP, half, feats), bf),
+            pltpu.VMEM((3, TP, count, hidden), bf),
+            pltpu.VMEM((3, TP, count, hidden), bf),
+            pltpu.VMEM((2, 2, TP, count, width), bf),
+            pltpu.VMEM((TP, count, feats), bf),
+            pltpu.VMEM((3, count, feats), bf),
+            pltpu.VMEM((3, half, feats), bf),
+            pltpu.VMEM((TP, half, feats), bf),
+            pltpu.VMEM((2, 3, half, feats), bf),
+            [pltpu.VMEM(s, bf) for s in grad_shapes],
+            pltpu.VMEM((3, q, feats), bf),
+            pltpu.VMEM((2, half, feats), bf),
+            pltpu.VMEM((2, 2, tile, hidden), jnp.float32),
+            pltpu.VMEM((2, tile, hidden), jnp.float32),
+            pltpu.VMEM((tile, hidden), bf),
+            pltpu.SemaphoreType.DMA((128,)),
+            pltpu.SemaphoreType.DMA((128,)),
+            pltpu.SemaphoreType.DMA((18,)),
+            pltpu.SemaphoreType.REGULAR,
+        ],
+        compiler_params=pltpu.CompilerParams(
+            collective_id=0, has_side_effects=True, vmem_limit_bytes=67043328
+        ),
+        name="step",
+    )(
+        late_input, early_mid, cotangent, early_input,
+        gain_second.reshape((1, -1)), gain_first.reshape((1, -1)),
+        shard_second, shard_first,
+    )
+    rows, second, first = outs[0], outs[1:4], outs[4:7]
+    grads = tuple(first) + tuple(second)
+    return (rows[0], rows[1], rows[2]) + tuple(
+        old + new.astype(jnp.float32) for old, new in zip(sums, grads)
+    )
 
 
 def normalize(values, gain_vector):
@@ -92,7 +710,7 @@
     return jnp.swapaxes(parts, 0, 1).reshape(joined.shape)
 
 
-def per_device(
+def per_device_general(
     late_input,
     early_input,
     early_mid,
@@ -124,10 +742,6 @@
     columns_second = join_columns(early_shares[0])
     columns_first = join_columns(early_shares[1])
     columns_cotangent = join_columns(early_shares[2])
-    weights_second, columns_second, columns_first, columns_cotangent = lax.optimization_barrier(
-        (weights_second, columns_second, columns_first, columns_cotangent)
-    )
-
     partial_second, pieces_second = block_backward(
         norm_second, cotangent, weights_second, width
     )
@@ -135,15 +749,11 @@
     mid_rows = backward_rows(norm_second, cotangent, gain_second, partial_second)
     mid_grad = join_rows(mid_rows)
     columns_mid = join_columns(share_columns(mid_rows))
-    weights_first, pieces_second, mid_grad, columns_mid = lax.optimization_barrier(
-        (weights_first, pieces_second, mid_grad, columns_mid)
-    )
     partial_first, pieces_first = block_backward(norm_first, mid_grad, weights_first, width)
     all_first = lax.all_gather(pieces_first, "fs", axis=0, tiled=True)
     late_mid = block_forward(late_input, gain_first, weights_first, width)
     input_grad = join_rows(backward_rows(norm_first, mid_grad, gain_first, partial_first))
     late_out = block_forward(late_mid, gain_second, weights_second, width)
-    all_second, late_out, input_grad = lax.optimization_barrier((all_second, late_out, input_grad))
 
     def collect(pieces, columns_in, columns_out, sums):
         return (
@@ -155,7 +765,6 @@
     new_second = collect(
         all_second, columns_second, columns_cotangent, (sum_gate_second, sum_up_second, sum_down_second)
     )
-    all_first, new_second = lax.optimization_barrier((all_first, new_second))
     new_first = collect(
         all_first, columns_first, columns_mid, (sum_gate_first, sum_up_first, sum_down_first)
     )
@@ -163,37 +772,12 @@
 
 
 def solution(mesh):
-    in_specs = (
-        P("fs", None),
-        P("fs", None),
-        P("fs", None),
-        P("fs", None),
-        P(),
-        P(),
-        P("fs", "tp"),
-        P("fs", "tp"),
-        P("tp", "fs"),
-        P("fs", "tp"),
-        P("fs", "tp"),
-        P("tp", "fs"),
-        P("fs", "tp"),
-        P("fs", "tp"),
-        P("tp", "fs"),
-        P("fs", "tp"),
-        P("fs", "tp"),
-        P("tp", "fs"),
-    )
-    out_specs = (
-        P("fs", None),
-        P("fs", None),
-        P("fs", None),
-        P("fs", "tp"),
-        P("fs", "tp"),
-        P("tp", "fs"),
-        P("fs", "tp"),
-        P("fs", "tp"),
-        P("tp", "fs"),
-    )
+    rows, up_down, down_up = P("fs", None), P("fs", "tp"), P("tp", "fs")
+    weights = (up_down, up_down, down_up)
+    in_specs = (rows,) * 4 + (P(), P()) + weights * 4
+    out_specs = (rows,) * 3 + weights * 2
+    line_of_four = mesh.shape["fs"] == PLANES * CORES and mesh.shape["tp"] == TP
+    body = per_device if line_of_four else per_device_general
     return jax.shard_map(
-        per_device, mesh=mesh, in_specs=in_specs, out_specs=out_specs, check_vma=False
-    )
+        body, mesh=mesh, in_specs=in_specs, out_specs=out_specs, check_vma=False
+    )

time: 317 us -> 240 us (0.76)
  Pallas kernels: 0 us -> 222 us
  blocking collectives: 119 us -> 0 us
  waiting for transfers between devices: 74.9 us -> 0 us
  matrix products: 56.6 us -> 0 us
  starting transfers between devices: 20.8 us -> 0 us
  between operations: 14.2 us -> 0.8 us
  other arithmetic: 16.6 us -> 6.93 us
  local copies, waits for them, and re-layouts: 13.9 us -> 9.47 us
    pallas_call x0 -> x1, Pallas kernels: none -> 222 us  [per_device(): pl.pallas_call(step_kernel, out_shape=[jax.ShapeDtypeStruct((3, count, fe...]
    all_gather x8 -> x0, blocking collectives: 85.4 us -> none  [join_rows(): return lax.all_gather(rows, 'tp', axis=0, tiled=True)]
    dot_general x16 -> x0, matrix products: 56.6 us -> none  [the longest x6 23.5 us: project(): return jnp.dot(rows, weights, preferred_element_type=jnp.float32)]
    all_gather x4 -> x0, waiting for transfers between devices: 54.4 us -> none  [the longest x2 48 us: gather_weights(): lax.all_gather(jnp.concatenate((gate, up, down.T), axis=1), 'fs', axis=0,...]
    all_to_all x1 -> x0, blocking collectives: 33.2 us -> none  [per_device(): lax.all_to_all(early_rows, 'fs', split_axis=2, concat_axis=1, tiled=True)]
    all_to_all x5 -> x0, starting transfers between devices: 20.7 us -> none  [the longest x4 17 us: sum_rows(): lax.all_to_all(partial.astype(jnp.bfloat16), 'tp', split_axis=0, concat_a...]
    all_to_all x5 -> x0, waiting for transfers between devices: 20.5 us -> none  [the longest x4 11.2 us: sum_rows(): lax.all_to_all(partial.astype(jnp.bfloat16), 'tp', split_axis=0, concat_a...]
    convert_element_type x10 -> x0, other arithmetic: 7.91 us -> none  [the longest x4 3.36 us: normalize(): widened = values.astype(jnp.float32)]
  transfers between devices with their start and end apart: 9 -> 0, of which waited for: 6 -> 0; matrix products, arithmetic and copies ran while one was open for 23% -> 0% of each run, Pallas kernels for 0% -> 0%
where the time goes in v1:
time: 240 us; the launch traced here: 239 us
  Pallas kernels  222 us (92%)
  local copies, waits for them, and re-layouts  9.47 us (4%)
  other arithmetic  6.93 us (3%)
    pallas_call x1, Pallas kernels, per_device(): pl.pallas_call(step_kernel, out_shape=[jax.ShapeDtypeStruct((3, count, fe...  222 us
    unnamed x34, local copies, waits for them, and re-layouts  6.82 us

profile of v1, /device:TPU:0, one launch (start us, length us, event | category | flops | bytes accessed | tf_op | source)
XLA Modules:
  0.0 239.3 jit_solution(3190571496485677302)
XLA Ops:
  0.6 0.0 copy-start.10
  0.7 0.0 copy-start.11
  0.7 0.0 copy-start.12
  0.7 2.4 pad_maximum_fusion.w2
  3.0 0.0 copy-done.10
  3.0 0.0 copy-done.11
  3.0 0.0 copy-done.12
  3.0 1.0 pad_maximum_fusion.1.w1
  4.1 222.1 %step.1 = (bf16[3,128,2048]{2,1,0:T(8,128)(2,1)}, bf16[256,704]{1,0:T(8,128)(2,1)}, bf16[256,704]{1,0:T(8,128)(2,1)}, bf16[704,256]{1,0:T(8,128)(2,1)}, bf16[256...) custom-call(bf16[128,2048]{1,0:T(8,128)(2,1)} %late_in.1, bf16[128,2048]{1,0:T(8,128)(2,1)} %mid_in.1, ...), custom_call_target="tpu_custom_call" | custom-call | tf_op jit(solution)/shard_map/step/pallas_call | solution.py:580
  226.2 0.0 copy-start.2
  226.2 0.0 copy-start.3
  226.2 2.7 %slice_bitcast_fusion = (bf16[128,2048]{1,0:T(8,128)(2,1)}, bf16[128,2048]{1,0:T(8,128)(2,1)}, bf16[128,2048]{1,0:T(8,128)(2,1)}) fusion(bf16[3,128,2048]{2,1,0:T(8,128)(2,1)} %get-tuple-element.16), kind=kLoop, calls=%fused_computation.8 | loop fusion | bytes 3145728 | tf_op jit(solution)/shard_map/squeeze | solution.py:622
  228.9 0.0 copy-start.7
  228.9 0.0 copy-done.2
  228.9 0.3 copy.28
  229.1 0.0 copy-done.3
  229.2 0.3 copy.27
  229.4 0.4 copy-done.7
  229.9 1.1 convert_add_fusion.2
  231.0 0.0 copy-start
  231.0 0.0 copy-start.1
  231.0 0.0 copy-start.8
  231.1 1.1 copy.31
  232.2 0.0 copy-start.9
  232.2 1.1 copy.32
  233.3 0.0 copy-done
  233.3 0.0 copy-done.1
  233.3 0.0 copy-done.8
  233.3 0.0 copy-done.9
  233.3 0.0 copy-start.4
  233.3 1.2 convert_add_fusion.4
  234.5 0.0 copy-start.5
  234.5 0.0 copy-start.6
  234.5 0.0 copy-done.4
  234.5 0.3 copy.30
  234.8 0.8 copy-done.5
  235.6 0.3 copy.29
  235.9 0.0 copy-done.6
  235.9 1.1 convert_add_fusion
  237.1 1.1 copy.33
  238.2 1.1 copy.34
Async XLA Ops:
  0.6 2.4 copy-start.10
  0.7 2.4 copy-start.11
  0.7 2.4 copy-start.12
  226.2 2.7 %copy-start.2 = (f32[256,704]{0,1:T(8,128)S(1)}, f32[256,704]{0,1:T(8,128)}, u32[]{:S(2)}) copy-start(f32[256,704]{0,1:T(8,128)} %param.31) | copy-start | bytes 2162692
  226.2 2.9 %copy-start.3 = (f32[256,704]{0,1:T(8,128)S(1)}, f32[256,704]{0,1:T(8,128)}, u32[]{:S(2)}) copy-start(f32[256,704]{0,1:T(8,128)} %param.30) | copy-start | bytes 2162692
  228.9 1.0 copy-start.7
  231.0 2.3 copy-start
  231.0 2.3 copy-start.1
  231.0 2.2 copy-start.8
  232.2 1.1 copy-start.9
  233.3 1.3 copy-start.4
  234.5 1.1 copy-start.5
  234.5 1.4 copy-start.6

commit v2 on v1

--- a/solution.py
+++ b/solution.py
@@ -28,8 +28,9 @@
 
 
 def step_kernel(
-    late_in, mid_in, cot_in, early_in, gain2, gain1, w2, w1,
-    out_rows, g20, g21, g22, g10, g11, g12,
+    late_in, mid_in, cot_in, early_in, gain2, gain1,
+    gate2, up2, down2, gate1, up1, down1,
+    late_mid, late_out, grad_in, grads2, grads1,
     weights, acts, late, normed, late_normed, pieces, pieces_in, cols_in,
     part, part_in2, part_in1, late_part, late_part_in, sent, back_rows, done_rows,
     acc, late_acc, late_hid, send_sems, recv_sems, local_sems, ack,
@@ -43,11 +44,11 @@
     q = late_in.shape[0] // TP
     rows = PLANES * q
     half = 2 * q
-    width = w2.shape[1]
-    hidden = w2.shape[0] // 3
+    hidden, width = down2.shape
     tile = TP * half
-    grads = ((g20, g21, g22), (g10, g11, g12))
-    shards = (w2, w1)
+    grads = (grads2, grads1)
+    shards = ((gate2, up2, down2), (gate1, up1, down1))
+    out_rows = (late_mid, late_out, grad_in)
     gains = (gain2, gain1)
     ids = {}
 
@@ -91,16 +92,19 @@
     pl.semaphore_wait(barrier, len(friends))
 
     mine = own_quarter(t)
-    z_items = []
-    for name, src, to in (
-        ("m", mid_in, lambda s: acts.at[0, 0, pl.ds(s * q, q)]),
-        ("c", cot_in, lambda s: acts.at[1, 0, pl.ds(s * q, q)]),
-    ):
-        z_items.append((name, src.at[mine], to))
-    z_items.append(("w0", w2, lambda s: weights.at[0, s]))
-    z_items.append(("e", early_in.at[mine], lambda s: acts.at[2, 0, pl.ds(s * q, q)]))
-    z_items.append(("l", late_in.at[mine], lambda s: late.at[0, 0, pl.ds(s * q, q)]))
-    z_items.append(("w1", w1, lambda s: weights.at[1, s]))
+    parts = [pl.ds(j * hidden, hidden) for j in range(3)]
+
+    def row_item(name, ref, store):
+        return (name, ref.at[mine], lambda s: store.at[pl.ds(s * q, q)])
+
+    def shard_item(b, j):
+        return (("w", b, j), shards[b][j], lambda s: weights.at[b, s, parts[j]])
+
+    z_items = [row_item("m", mid_in, acts.at[0, 0]), row_item("c", cot_in, acts.at[1, 0])]
+    z_items += [shard_item(0, 0), shard_item(0, 1)]
+    z_items += [row_item("e", early_in, acts.at[2, 0]), row_item("l", late_in, late.at[0, 0])]
+    z_items += [shard_item(0, 2)]
+    z_items += [shard_item(1, j) for j in range(3)]
     z_base = {}
     for name, _, _ in z_items:
         z_base[name] = sem((name, 0))
@@ -129,7 +133,7 @@
     out_dev = device(near, core, t)
 
     def grad_back(b, j):
-        return remote(sent[3 * b + j], grads[b][j], sem(("g", b, j)), out_dev)
+        return remote(sent.at[b, j], grads[b].at[j], sem(("g", b, j)), out_dev)
 
     def row_source(k):
         return (late.at[1, 0], done_rows.at[0], done_rows.at[1])[k]
@@ -138,11 +142,11 @@
         return remote(row_source(k).at[pl.ds(q, q)], back_rows.at[k], sem(("r", k)), out_dev)
 
     def deliver(k, m, src):
-        return remote(src, out_rows.at[k, mine], sem(("d", k, m)), device(z, core, column(m)))
+        return remote(src, out_rows[k].at[mine], sem(("d", k, m)), device(z, core, column(m)))
 
     def deliver_wait(k, m):
         other = column(m)
-        dst = out_rows.at[k, own_quarter(other)]
+        dst = out_rows[k].at[own_quarter(other)]
         remote(dst, dst, sem(("d", k, m)), device(z, core, other)).wait_recv()
 
     for b in range(2):
@@ -157,11 +161,11 @@
     def _():
         for copy in outer_sends():
             copy.start()
-        for k in (0, 1, 2):
+        for k in (0, 2, 1):
             rows_back(k).wait_recv()
             for m in range(1, TP):
                 deliver(k, m, back_rows.at[k]).start()
-            out_rows[k, mine, :] = back_rows[k]
+            out_rows[k][mine, :] = back_rows[k]
         for copy in outer_sends():
             copy.wait_send()
         for b in range(2):
@@ -178,32 +182,35 @@
             copy.start()
         peer_dev = device(z, peer, t)
 
-        def shard_local(b):
-            return local(shards[b], weights.at[b, 0], b)
+        def shard_local(b, j):
+            return local(shards[b][j], weights.at[b, 0, parts[j]], 3 * b + j)
 
         w_base = []
         for b in range(2):
-            w_base.append(sem(("p", b, 0)))
-            for s in range(1, 4):
-                sem(("p", b, s))
-
-        def shard_forward(b, s, src):
-            return remote(src, weights.at[b, 4 + s], w_base[b] + s, peer_dev)
+            w_base.append([])
+            for j in range(3):
+                w_base[b].append(sem(("p", b, j, 0)))
+                for s in range(1, 4):
+                    sem(("p", b, j, s))
+
+        def shard_forward(b, j, s, src):
+            return remote(src, weights.at[b, 4 + s, parts[j]], w_base[b][j] + s, peer_dev)
 
         def row_locals(a):
             src = (mid_in, cot_in, early_in, late_in)[a]
             out = []
             for m in range(TP):
                 dst = late.at[0, m, pl.ds(0, q)] if a == 3 else acts.at[a, m, pl.ds(0, q)]
-                out.append(local(src.at[own_quarter(column(m))], dst, 2 + TP * a + m))
+                out.append(local(src.at[own_quarter(column(m))], dst, 6 + TP * a + m))
             return out
 
-        for b in range(2):
-            shard_local(b).start()
-            shard_forward(b, 0, shards[b]).start()
         for a in range(4):
             for copy in row_locals(a):
                 copy.start()
+        for b in range(2):
+            for j in range(3):
+                shard_local(b, j).start()
+                shard_forward(b, j, 0, shards[b][j]).start()
 
         def spread_rows(a):
             src = (acts.at[a, 0], late.at[0, 0])[a == 3].at[pl.ds(q, q if a == 3 else 3 * q)]
@@ -244,28 +251,30 @@
             at = pl.ds(pl.multiple_of(h * half, half), half)
             return ref[:, at, cols].reshape(tile, width)
 
+        def take_part(b, j, slot, other):
+            @pl.when((slot == 0) & (other == 0))
+            def _():
+                shard_local(b, j).wait()
+
+            @pl.when((slot > 0) & (other == 0))
+            def _():
+                ref = weights.at[b, slot, parts[j]]
+                remote(ref, ref, z_base[("w", b, j)] + slot, mid_target).wait_recv()
+                shard_forward(b, j, slot, ref).start()
+
+            @pl.when(other == 1)
+            def _():
+                ref = weights.at[b, 4 + slot, parts[j]]
+                remote(ref, ref, w_base[b][j] + slot, peer_dev).wait_recv()
+
         def pre_block(b):
             acc[...] = jnp.zeros_like(acc)
 
             @pl.loop(0, 8)
             def _(i):
                 slot, other = i // 2, i % 2
-
-                @pl.when(i == 0)
-                def _():
-                    shard_local(b).wait()
-
-                @pl.when((i > 0) & (other == 0))
-                def _():
-                    ref = weights.at[b, slot]
-                    remote(ref, ref, z_base["w%d" % b] + slot, mid_target).wait_recv()
-                    shard_forward(b, slot, ref).start()
-
-                @pl.when(other == 1)
-                def _():
-                    ref = weights.at[b, 4 + slot]
-                    remote(ref, ref, w_base[b] + slot, peer_dev).wait_recv()
-
+                for j in range(2):
+                    take_part(b, j, slot, other)
                 at = slot + 4 * other
                 cols = feature(slot, other)
 
@@ -273,34 +282,42 @@
                 def _(h):
                     piece = rows_of(normed, h, cols)
                     for j in range(2):
-                        w = weights[b, at, pl.ds(j * hidden, hidden), :]
-                        acc[j, h] += mm(piece, w, NT)
-
-        def pieces_block(b):
+                        acc[j, h] += mm(piece, weights[b, at, parts[j], :], NT)
+
+        def take_down(b):
+            @pl.loop(0, 8)
+            def _(i):
+                take_part(b, 2, i // 2, i % 2)
+
+        def down_block(b, take):
             cots = acts.at[2 * b + 1]
-
-            @pl.loop(0, 2)
-            def _(h):
-                late_acc[0] = jnp.zeros_like(late_acc[0])
-
-                @pl.loop(0, 8)
-                def _(i):
-                    cols = feature(i % 4, i // 4)
-                    w = weights[b, i, pl.ds(2 * hidden, hidden), :]
-                    late_acc[0] += mm(rows_of(cots, h, cols), w, NT)
-
-                @pl.loop(0, TP)
-                def _(m):
-                    at = pl.ds(pl.multiple_of(m * half, half), half)
-                    to = pl.ds(pl.multiple_of(h * half, half), half)
-                    gate, up = acc[0, h, at, :], acc[1, h, at, :]
-                    grad = 0.5 * late_acc[0, at, :]
-                    sig = 1.0 / (1.0 + jnp.exp(-gate))
-                    act = gate * sig
-                    turn = sig * (1.0 + gate * (1.0 - sig))
-                    pieces[0, m, to, :] = (grad * up * turn).astype(jnp.bfloat16)
-                    pieces[1, m, to, :] = (grad * act).astype(jnp.bfloat16)
-                    pieces[2, m, to, :] = (act * up).astype(jnp.bfloat16)
+            late_acc[...] = jnp.zeros_like(late_acc)
+
+            @pl.loop(0, 8)
+            def _(i):
+                slot, other = i // 2, i % 2
+                if take:
+                    take_part(b, 2, slot, other)
+                cols = feature(slot, other)
+
+                @pl.loop(0, 2)
+                def _(h):
+                    w = weights[b, slot + 4 * other, parts[2], :]
+                    late_acc[h] += mm(rows_of(cots, h, cols), w, NT)
+
+        def pieces_block(h):
+            @pl.loop(0, TP)
+            def _(m):
+                at = pl.ds(pl.multiple_of(m * half, half), half)
+                to = pl.ds(pl.multiple_of(h * half, half), half)
+                gate, up = acc[0, h, at, :], acc[1, h, at, :]
+                grad = 0.5 * late_acc[h, at, :]
+                sig = 1.0 / (1.0 + jnp.exp(-gate))
+                act = gate * sig
+                turn = sig * (1.0 + gate * (1.0 - sig))
+                pieces[0, m, to, :] = (grad * up * turn).astype(jnp.bfloat16)
+                pieces[1, m, to, :] = (grad * act).astype(jnp.bfloat16)
+                pieces[2, m, to, :] = (act * up).astype(jnp.bfloat16)
 
         def swaps(b):
             out = []
@@ -314,89 +331,73 @@
                     )
             return out
 
-        def part_copy(b, h, m, base):
-            at = pl.ds(pl.multiple_of(h * half, half), half)
-            dst = (part_in2, part_in1)[b]
+        def part_rows(b, r):
+            size = half if b == 0 else q
+            return pl.ds(r * size, size)
+
+        def part_copy(b, r, m):
+            at = part_rows(b, r)
             return remote(
-                part.at[m, at], dst.at[m - 1, at], base + h * 3 + (m - 1),
+                part.at[m, at], (part_in2, part_in1)[b].at[m - 1, at], sem(("n", b, r, m)),
                 device(z, core, column(m)),
             )
 
-        part_base = []
-        for b in range(2):
-            part_base.append(sem(("n", b, 0)))
-            for i in range(1, 6):
-                sem(("n", b, i))
-
-        def grad_part(b):
-            @pl.loop(0, 2 - b)
-            def _(h):
-                at = pl.ds(pl.multiple_of(h * half, half), half)
-
-                @pl.loop(0, 8)
-                def _(i):
-                    cols = feature(i % 4, i // 4)
-                    total = None
-                    for j in range(2):
-                        left = pieces[j, :, at, :].reshape(tile, hidden)
-                        w = weights[b, i, pl.ds(j * hidden, hidden), :]
-                        one = mm(left, w, NN)
-                        total = one if j == 0 else total + one
-                    part[:, at, cols] = total.astype(jnp.bfloat16).reshape(TP, half, width)
-
-                for m in range(1, TP):
-                    part_copy(b, h, m, part_base[b]).start()
+        def grad_part(b, h):
+            at = pl.ds(h * half, half)
+
+            @pl.loop(0, 8)
+            def _(i):
+                cols = feature(i % 4, i // 4)
+                total = None
+                for j in range(2):
+                    left = pieces[j, :, at, :].reshape(tile, hidden)
+                    one = mm(left, weights[b, i, parts[j], :], NN)
+                    total = one if j == 0 else total + one
+                part[:, at, cols] = total.astype(jnp.bfloat16).reshape(TP, half, width)
 
         def fold(b):
             for copy in swaps(b):
                 copy.wait_recv()
             tokens = TP * rows
             cots = acts.at[2 * b + 1]
-            for k in range(2):
+            for k in (1, 0):
                 cols = feature(k, 0)
-                outs = grads[b] if k == 0 else sent[3 * b : 3 * b + 3]
-                a0 = normed[:, :, cols].reshape(tokens, width)
-                a1 = cols_in[0, k].reshape(tokens, width)
-                for j in range(2):
-                    one = mm(a0, pieces[j].reshape(tokens, hidden), TN)
-                    one = one + mm(a1, pieces_in[j].reshape(tokens, hidden), TN)
-                    outs[j][...] = one.astype(jnp.bfloat16)
-                one = mm(pieces[2].reshape(tokens, hidden), cots[:, :, cols].reshape(tokens, width), TN)
-                one = one + mm(
-                    pieces_in[2].reshape(tokens, hidden), cols_in[1, k].reshape(tokens, width), TN
+                out = sent.at[b] if k == 1 else grads[b]
+                sides = (
+                    (normed[:, :, cols].reshape(tokens, width), cols_in[0, k].reshape(tokens, width)),
+                    (cots[:, :, cols].reshape(tokens, width), cols_in[1, k].reshape(tokens, width)),
                 )
-                outs[2][...] = (0.5 * one).astype(jnp.bfloat16)
-            for j in range(3):
-                grad_back(b, j).start()
-
-        def rows_grad(b, h, store):
+                for j in range(3):
+                    own, other = sides[j // 2]
+                    one = mm(pieces[j].reshape(tokens, hidden), own, TN)
+                    one = one + mm(pieces_in[j].reshape(tokens, hidden), other, TN)
+                    out[j] = (one if j < 2 else 0.5 * one).astype(jnp.bfloat16)
+                    if k == 1 and (b == 0 or j < 2):
+                        grad_back(b, j).start()
+
+        def rows_grad(b, r, out):
+            for m in range(1, TP):
+                part_copy(b, r, m).wait_recv()
             arrived = (part_in2, part_in1)[b]
-
-            @pl.loop(0, 2)
-            def _(i):
-                at = pl.ds(pl.multiple_of(h * half + i * q, q), q)
-                total = part[0, at, :].astype(jnp.float32)
-                for m in range(1, TP):
-                    total = total + arrived[m - 1, at, :].astype(jnp.float32)
-                wide, factor = norm_parts(acts[2 * b, 0, at, :])
-                scaled = total * gains[b][...]
-                unit = wide * factor
-                inner_mean = jnp.mean(scaled * unit, axis=-1, keepdims=True)
-                cot = acts[2 * b + 1, 0, at, :].astype(jnp.float32)
-                store(at, (cot + factor * (scaled - unit * inner_mean)).astype(jnp.bfloat16))
-
-        def mid_copy(h, m, base):
-            at = pl.ds(pl.multiple_of(h * half, half), half)
+            at = part_rows(b, r)
+            total = part[0, at, :].astype(jnp.float32)
+            for m in range(1, TP):
+                total = total + arrived[m - 1, at, :].astype(jnp.float32)
+            wide, factor = norm_parts(acts[2 * b, 0, at, :])
+            scaled = total * gains[b][...]
+            unit = wide * factor
+            inner_mean = jnp.mean(scaled * unit, axis=-1, keepdims=True)
+            cot = acts[2 * b + 1, 0, at, :].astype(jnp.float32)
+            out[at, :] = (cot + factor * (scaled - unit * inner_mean)).astype(jnp.bfloat16)
+
+        def mid_copy(h, m):
+            at = pl.ds(h * half, half)
             return remote(
-                acts.at[3, 0, at], acts.at[3, m, at], base + h * 3 + (m - 1),
+                acts.at[3, 0, at], acts.at[3, m, at], sem(("a", h, m)),
                 device(z, core, column(m)),
             )
 
-        mid_base = sem(("a", 0))
-        for i in range(1, 6):
-            sem(("a", i))
-
-        def late_block(b, n):
+        def late_block(b, n, take):
             @pl.loop(0, TP * 2)
             def _(i):
                 at = pl.ds(pl.multiple_of((i % 2) * q, q), q)
@@ -410,41 +411,40 @@
                 cols = feature(i % 4, i // 4)
                 piece = late_normed[:, :, cols].reshape(tile, width)
                 for j in range(2):
-                    w = weights[b, i, pl.ds(j * hidden, hidden), :]
-                    late_acc[j] += mm(piece, w, NT)
+                    late_acc[j] += mm(piece, weights[b, i, parts[j], :], NT)
 
             gate = late_acc[0]
             hid = (gate / (1.0 + jnp.exp(-gate)) * late_acc[1]).astype(jnp.bfloat16)
             late_hid[...] = hid
+            if take:
+                take_down(b)
 
             @pl.loop(0, 8)
             def _(i):
                 cols = feature(i % 4, i // 4)
-                w = weights[b, i, pl.ds(2 * hidden, hidden), :]
-                one = mm(late_hid[...], w, NN).astype(jnp.bfloat16)
+                one = mm(late_hid[...], weights[b, i, parts[2], :], NN).astype(jnp.bfloat16)
                 late_part[:, :, cols] = one.reshape(TP, half, width)
 
-            for m in range(1, TP):
-                late_copy(n, m).start()
-
-        def late_copy(n, m):
+            for r in (1, 0):
+                for m in range(1, TP):
+                    late_copy(n, r, m).start()
+
+        def late_copy(n, r, m):
+            at = pl.ds(r * q, q)
             return remote(
-                late_part.at[m], late_part_in.at[n, m - 1], sem(("h", n, m)),
+                late_part.at[m, at], late_part_in.at[n, m - 1, at], sem(("h", n, r, m)),
                 device(z, core, column(m)),
             )
 
-        def late_sum(n, store):
-            for m in range(1, TP):
-                late_copy(n, m).wait_recv()
-
-            @pl.loop(0, 2)
-            def _(i):
-                at = pl.ds(pl.multiple_of(i * q, q), q)
-                total = late_part[0, at, :].astype(jnp.float32)
-                for m in range(1, TP):
-                    total = total + late_part_in[n, m - 1, at, :].astype(jnp.float32)
-                value = late[n, 0, at, :].astype(jnp.float32) + 0.5 * total
-                store(at, value.astype(jnp.bfloat16))
+        def late_sum(n, r, out):
+            for m in range(1, TP):
+                late_copy(n, r, m).wait_recv()
+            at = pl.ds(r * q, q)
+            total = late_part[0, at, :].astype(jnp.float32)
+            for m in range(1, TP):
+                total = total + late_part_in[n, m - 1, at, :].astype(jnp.float32)
+            value = late[n, 0, at, :].astype(jnp.float32) + 0.5 * total
+            out[at, :] = value.astype(jnp.bfloat16)
 
         def late_spread(m):
             return remote(
@@ -455,23 +455,22 @@
         normalize_block(0)
         pre_block(0)
         rows_ready(1)
-        pieces_block(0)
+        gather_rows(2, 4)
+        gather_rows(3, 5)
+        down_block(0, True)
+        for h in range(2):
+            pieces_block(h)
+            grad_part(0, h)
+            for m in range(1, TP):
+                part_copy(0, h, m).start()
         for copy in swaps(0):
             copy.start()
-        grad_part(0)
-        gather_rows(2, 3)
-        gather_rows(3, 4)
-        fold(0)
-
-        def keep_mid(at, value):
-            acts[3, 0, at, :] = value
-
         for h in range(2):
-            for m in range(1, TP):
-                part_copy(0, h, m, part_base[0]).wait_recv()
-            rows_grad(0, h, keep_mid)
-            for m in range(1, TP):
-                mid_copy(h, m, mid_base).start()
+            rows_grad(0, h, acts.at[3, 0])
+            for m in range(1, TP):
+                mid_copy(h, m).start()
+            if h == 0:
+                fold(0)
         for copy in swaps(0):
             copy.wait_send()
         pl.semaphore_signal(ack, inc=1, device_id=peer_dev, device_id_type=pl.DeviceIdType.MESH)
@@ -480,57 +479,64 @@
         normalize_block(1)
         pre_block(1)
         rows_ready(3)
-        late_block(1, 0)
+        late_block(1, 0, True)
         for h in range(2):
             for m in range(1, TP):
-                mid_copy(h, m, mid_base).wait_recv()
-        pieces_block(1)
+                mid_copy(h, m).wait_recv()
+        down_block(1, False)
+
+        @pl.loop(0, 2)
+        def _(h):
+            pieces_block(h)
+
         pl.semaphore_wait(ack, 1)
         for copy in swaps(1):
             copy.start()
-        for h in range(2):
-            for m in range(1, TP):
-                part_copy(0, h, m, part_base[0]).wait_send()
-        grad_part(1)
-
-        def keep_late(at, value):
-            late[1, 0, at, :] = value
-
-        late_sum(0, keep_late)
+        for r in range(2):
+            for m in range(1, TP):
+                part_copy(0, r, m).wait_send()
+        grad_part(1, 0)
+        late_rows = late.at[1, 0]
+        late_sum(0, 1, late_rows)
+        late_sum(0, 0, late_rows)
         for m in range(1, TP):
             late_spread(m).start()
         rows_back(0).start()
+        for r in (1, 0):
+            for m in range(1, TP):
+                part_copy(1, r, m).start()
         fold(1)
         for m in range(1, TP):
             late_spread(m).wait_recv()
-            late_copy(0, m).wait_send()
-        late_block(0, 1)
-        for m in range(1, TP):
-            part_copy(1, 0, m, part_base[1]).wait_recv()
-
-        def keep_done(index):
-            def store(at, value):
-                done_rows[index, at, :] = value
-
-            return store
-
-        rows_grad(1, 0, keep_done(1))
+            for r in range(2):
+                late_copy(0, r, m).wait_send()
+        late_block(0, 1, False)
+        for m in range(TP):
+            late_mid[own_quarter(column(m)), :] = late[1, m, pl.ds(0, q), :]
+
+        def finish(k):
+            src = row_source(k).at[pl.ds(0, q)]
+            for m in range(1, TP):
+                deliver(k, m, src).start()
+            out_rows[k][mine, :] = src[...]
+
+        rows_grad(1, 1, done_rows.at[1])
         rows_back(2).start()
-        late_sum(1, keep_done(0))
+        rows_grad(1, 0, done_rows.at[1])
+        late_sum(1, 1, done_rows.at[0])
         rows_back(1).start()
-        for k in range(3):
-            src = row_source(k).at[pl.ds(0, q)]
-            for m in range(1, TP):
-                deliver(k, m, src).start()
-            out_rows[k, mine, :] = src[...]
+        grad_back(1, 2).start()
+        finish(2)
+        late_sum(1, 0, done_rows.at[0])
+        finish(1)
 
         for copy in inner_sends():
             copy.wait_send()
         for b in range(2):
-            for s in range(4):
-                src = shards[b] if s == 0 else weights.at[b, s]
-                shard_forward(b, s, src).wait_send()
             for j in range(3):
+                for s in range(4):
+                    src = shards[b][j] if s == 0 else weights.at[b, s, parts[j]]
+                    shard_forward(b, j, s, src).wait_send()
                 grad_back(b, j).wait_send()
         for a in range(4):
             for copy in spread_rows(a):
@@ -538,16 +544,26 @@
         for copy in swaps(1):
             copy.wait_send()
         for m in range(1, TP):
-            for h in range(2):
-                mid_copy(h, m, mid_base).wait_send()
-            part_copy(1, 0, m, part_base[1]).wait_send()
+            for r in range(2):
+                mid_copy(r, m).wait_send()
+                part_copy(1, r, m).wait_send()
+                late_copy(1, r, m).wait_send()
             late_spread(m).wait_send()
-            late_copy(1, m).wait_send()
         for k in range(3):
             rows_back(k).wait_send()
-            for m in range(1, TP):
-                deliver(k, m, row_source(k).at[pl.ds(0, q)]).wait_send()
-                deliver_wait(k, m)
+            if k > 0:
+                for m in range(1, TP):
+                    deliver(k, m, row_source(k).at[pl.ds(0, q)]).wait_send()
+                    deliver_wait(k, m)
+
+
+def add_kernel(r0, r1, r2, grads2, grads1, *refs):
+    olds, outs = refs[:6], refs[6:]
+    for src, dst in zip((r0, r1, r2), outs[:3]):
+        dst[...] = src[...]
+    for j in range(6):
+        grads = (grads1, grads2)[j // 3]
+        outs[3 + j][...] = olds[j][...] + grads[j % 3].astype(jnp.float32)
 
 
 def per_device(
@@ -571,18 +587,15 @@
     half = 2 * q
     tile = TP * half
     bf = jnp.bfloat16
-    shard_second = jnp.concatenate((gate_second.T, up_second.T, down_second), axis=0)
-    shard_first = jnp.concatenate((gate_first.T, up_first.T, down_first), axis=0)
-    wide, tall = (width, hidden), (hidden, width)
-    grad_shapes = [wide, wide, tall] * 2
     anywhere = pl.BlockSpec(memory_space=pl.ANY)
     in_vmem = pl.BlockSpec(memory_space=pltpu.VMEM)
+    rows_shape = jax.ShapeDtypeStruct((count, feats), bf)
+    grads_shape = jax.ShapeDtypeStruct((3, hidden, width), bf)
     outs = pl.pallas_call(
         step_kernel,
-        out_shape=[jax.ShapeDtypeStruct((3, count, feats), bf)]
-        + [jax.ShapeDtypeStruct(s, bf) for s in grad_shapes],
-        in_specs=[anywhere] * 4 + [in_vmem] * 2 + [anywhere] * 2,
-        out_specs=[in_vmem] * 7,
+        out_shape=[rows_shape] * 3 + [grads_shape] * 2,
+        in_specs=[anywhere] * 4 + [in_vmem] * 2 + [anywhere] * 6,
+        out_specs=[in_vmem] * 5,
         scratch_shapes=[
             pltpu.VMEM((2, 8, 3 * hidden, width), bf),
             pltpu.VMEM((4, TP, count, feats), bf),
@@ -597,15 +610,15 @@
             pltpu.VMEM((3, half, feats), bf),
             pltpu.VMEM((TP, half, feats), bf),
             pltpu.VMEM((2, 3, half, feats), bf),
-            [pltpu.VMEM(s, bf) for s in grad_shapes],
+            pltpu.VMEM((2, 3, hidden, width), bf),
             pltpu.VMEM((3, q, feats), bf),
             pltpu.VMEM((2, half, feats), bf),
             pltpu.VMEM((2, 2, tile, hidden), jnp.float32),
             pltpu.VMEM((2, tile, hidden), jnp.float32),
             pltpu.VMEM((tile, hidden), bf),
-            pltpu.SemaphoreType.DMA((128,)),
-            pltpu.SemaphoreType.DMA((128,)),
-            pltpu.SemaphoreType.DMA((18,)),
+            pltpu.SemaphoreType.DMA((160,)),
+            pltpu.SemaphoreType.DMA((160,)),
+            pltpu.SemaphoreType.DMA((22,)),
             pltpu.SemaphoreType.REGULAR,
         ],
         compiler_params=pltpu.CompilerParams(
@@ -615,13 +628,24 @@
     )(
         late_input, early_mid, cotangent, early_input,
         gain_second.reshape((1, -1)), gain_first.reshape((1, -1)),
-        shard_second, shard_first,
+        gate_second.T, up_second.T, down_second,
+        gate_first.T, up_first.T, down_first,
     )
-    rows, second, first = outs[0], outs[1:4], outs[4:7]
-    grads = tuple(first) + tuple(second)
-    return (rows[0], rows[1], rows[2]) + tuple(
-        old + new.astype(jnp.float32) for old, new in zip(sums, grads)
-    )
+    tall = [old.T if j % 3 < 2 else old for j, old in enumerate(sums)]
+    steps = 4
+    row_spec = pl.BlockSpec((count // steps, feats), lambda i: (i, 0))
+    sum_spec = pl.BlockSpec((hidden // steps, width), lambda i: (i, 0))
+    grad_spec = pl.BlockSpec((3, hidden // steps, width), lambda i: (0, i, 0))
+    done = pl.pallas_call(
+        add_kernel,
+        grid=(steps,),
+        out_shape=[rows_shape] * 3 + [jax.ShapeDtypeStruct((hidden, width), jnp.float32)] * 6,
+        in_specs=[row_spec] * 3 + [grad_spec] * 2 + [sum_spec] * 6,
+        out_specs=[row_spec] * 3 + [sum_spec] * 6,
+        name="add",
+    )(*outs, *tall)
+    fresh = [new.T if j % 3 < 2 else new for j, new in enumerate(done[3:])]
+    return tuple(done[:3]) + tuple(fresh)
 
 
 def normalize(values, gain_vector):

time: 240 us -> 201 us (0.84)
  Pallas kernels: 222 us -> 197 us
  local copies, waits for them, and re-layouts: 9.47 us -> 0 us
  other arithmetic: 6.93 us -> 0 us
    pallas_call x1 -> x2, Pallas kernels: 222 us -> 197 us  [the longest x1 191 us: per_device(): pl.pallas_call(step_kernel, out_shape=[rows_shape] * 3 + [grads_shape] *...]
    unnamed x34 -> x0, local copies, waits for them, and re-layouts: 6.82 us -> none
    add x3 -> x0, other arithmetic: 3.53 us -> none  [per_device(): old + new.astype(jnp.float32)]
    concatenate x2 -> x0, other arithmetic: 3.4 us -> none  [the longest x1 2.35 us: per_device(): jnp.concatenate((gate_second.T, up_second.T, down_second), axis=0)]
    squeeze x1 -> x0, local copies, waits for them, and re-layouts: 2.65 us -> none  [per_device(): rows[2]]
where the time goes in v2:
time: 201 us; the launch traced here: 198 us
  Pallas kernels  197 us (98%)
    pallas_call x1, Pallas kernels, per_device(): pl.pallas_call(step_kernel, out_shape=[rows_shape] * 3 + [grads_shape] *...  191 us
    pallas_call x1, Pallas kernels, per_device(): pl.pallas_call(add_kernel, grid=(steps,), out_shape=[rows_shape] * 3 + [j...  6.14 us

profile of v2, /device:TPU:0, one launch (start us, length us, event | category | flops | bytes accessed | tf_op | source)
XLA Modules:
  0.0 198.0 jit_solution(14963488733222528657)
XLA Ops:
  0.6 191.2 %step.1 = (bf16[128,2048]{1,0:T(8,128)(2,1)}, bf16[128,2048]{1,0:T(8,128)(2,1)}, bf16[128,2048]{1,0:T(8,128)(2,1)}, bf16[3,704,256]{2,1,0:T(8,128)(2,1)}, bf16[3,704,256]{2,1,0:T(8,128)(2,1)}) custom-call(bf16[128,2048]{1,0:T(8,128)(2,1)} %late_in.1, bf16[128,2048]{1,0:T(8,128)(2,1)} %mid_in.1, bf16[128,2048]{1,0:T(8,128)(2,1)} %cot_in.1, ...), custom_call_target="tpu_custom_call" | custom-call | tf_op jit(solution)/shard_map/step/pallas_call | solution.py:594
  191.9 6.1 %add.1 = (bf16[128,2048]{1,0:T(8,128)(2,1)}, bf16[128,2048]{1,0:T(8,128)(2,1)}, bf16[128,2048]{1,0:T(8,128)(2,1)}, f32[704,256]{1,0:T(8,128)}, f32[704,256]{1,0:...) custom-call(bf16[128,2048]{1,0:T(8,128)(2,1)} %get-tuple-element.23.r0, ...), custom_call_target="tpu_custom_call" | custom-call | tf_op jit(solution)/shard_map/add/pallas_call | solution.py:639

commit v3 on v2

--- a/solution.py
+++ b/solution.py
@@ -33,7 +33,7 @@
     late_mid, late_out, grad_in, grads2, grads1,
     weights, acts, late, normed, late_normed, pieces, pieces_in, cols_in,
     part, part_in2, part_in1, late_part, late_part_in, sent, back_rows, done_rows,
-    acc, late_acc, late_hid, send_sems, recv_sems, local_sems, ack,
+    own_grads, acc, late_acc, late_hid, send_sems, recv_sems, local_sems, ack,
 ):
     f, t = lax.axis_index("fs"), lax.axis_index("tp")
     z, core = f // CORES, f % CORES
@@ -144,6 +144,9 @@
     def deliver(k, m, src):
         return remote(src, out_rows[k].at[mine], sem(("d", k, m)), device(z, core, column(m)))
 
+    def keep_rows(k, src):
+        return local(src, out_rows[k].at[mine], 22 + k)
+
     def deliver_wait(k, m):
         other = column(m)
         dst = out_rows[k].at[own_quarter(other)]
@@ -165,9 +168,11 @@
             rows_back(k).wait_recv()
             for m in range(1, TP):
                 deliver(k, m, back_rows.at[k]).start()
-            out_rows[k][mine, :] = back_rows[k]
+            keep_rows(k, back_rows.at[k]).start()
         for copy in outer_sends():
             copy.wait_send()
+        for k in range(3):
+            keep_rows(k, back_rows.at[k]).wait()
         for b in range(2):
             for j in range(3):
                 grad_back(b, j).wait_recv()
@@ -267,10 +272,11 @@
                 ref = weights.at[b, 4 + slot, parts[j]]
                 remote(ref, ref, w_base[b][j] + slot, peer_dev).wait_recv()
 
-        def pre_block(b):
-            acc[...] = jnp.zeros_like(acc)
-
-            @pl.loop(0, 8)
+        def pre_block(b, first, end):
+            if first == 0:
+                acc[...] = jnp.zeros_like(acc)
+
+            @pl.loop(first, end)
             def _(i):
                 slot, other = i // 2, i % 2
                 for j in range(2):
@@ -284,26 +290,22 @@
                     for j in range(2):
                         acc[j, h] += mm(piece, weights[b, at, parts[j], :], NT)
 
-        def take_down(b):
+        def down_shard(b, slot, other):
+            cots = acts.at[2 * b + 1]
+            cols = feature(slot, other)
+
+            @pl.loop(0, 2)
+            def _(h):
+                w = weights[b, slot + 4 * other, parts[2], :]
+                late_acc[h] += mm(rows_of(cots, h, cols), w, NT)
+
+        def down_block(b):
+            late_acc[...] = jnp.zeros_like(late_acc)
+
             @pl.loop(0, 8)
             def _(i):
                 take_part(b, 2, i // 2, i % 2)
-
-        def down_block(b, take):
-            cots = acts.at[2 * b + 1]
-            late_acc[...] = jnp.zeros_like(late_acc)
-
-            @pl.loop(0, 8)
-            def _(i):
-                slot, other = i // 2, i % 2
-                if take:
-                    take_part(b, 2, slot, other)
-                cols = feature(slot, other)
-
-                @pl.loop(0, 2)
-                def _(h):
-                    w = weights[b, slot + 4 * other, parts[2], :]
-                    late_acc[h] += mm(rows_of(cots, h, cols), w, NT)
+                down_shard(b, i // 2, i % 2)
 
         def pieces_block(h):
             @pl.loop(0, TP)
@@ -331,16 +333,47 @@
                     )
             return out
 
-        def part_rows(b, r):
-            size = half if b == 0 else q
-            return pl.ds(r * size, size)
-
-        def part_copy(b, r, m):
-            at = part_rows(b, r)
+        def part_copy(r, m):
+            at = pl.ds(r * q, q)
             return remote(
-                part.at[m, at], (part_in2, part_in1)[b].at[m - 1, at], sem(("n", b, r, m)),
+                part.at[m, at], part_in1.at[m - 1, at], sem(("n", r, m)),
                 device(z, core, column(m)),
             )
+
+        lanes = (pl.ds(0, normed.shape[2] // 2), pl.ds(normed.shape[2] // 2, normed.shape[2] // 2))
+
+        def part_first(h, columns=(1, 2), kinds=(0, 1)):
+            at = pl.ds(h * half, half)
+            out = []
+            for m in columns:
+                for kind in kinds:
+                    block, slot = ((m, m - 1), (3, 2))[kind]
+                    out.append(
+                        remote(
+                            part.at[block, at, lanes[m - 1]], part_in2.at[slot, at, lanes[m - 1]],
+                            sem(("o", h, m, slot)), device(z, core, column(m)),
+                        )
+                    )
+            return out
+
+        def part_second(h, columns=(1, 2)):
+            at = pl.ds(h * half, half)
+            return [
+                remote(
+                    part.at[3 - m, at, lanes[m - 1]], part_in2.at[2 - m, at, lanes[m - 1]],
+                    sem(("t", h, m)), device(z, core, column(3 - m)),
+                )
+                for m in columns
+            ]
+
+        def part_merge(h):
+            at = pl.ds(h * half, half)
+            for m in (1, 2):
+                part_first(h, (m,), (1,))[0].wait_recv()
+                mine_too = part[3 - m, at, lanes[m - 1]].astype(jnp.float32)
+                other = part_in2[2, at, lanes[m - 1]].astype(jnp.float32)
+                part[3 - m, at, lanes[m - 1]] = (mine_too + other).astype(jnp.bfloat16)
+                part_second(h, (m,))[0].start()
 
         def grad_part(b, h):
             at = pl.ds(h * half, half)
@@ -362,7 +395,7 @@
             cots = acts.at[2 * b + 1]
             for k in (1, 0):
                 cols = feature(k, 0)
-                out = sent.at[b] if k == 1 else grads[b]
+                out = (own_grads, sent)[k].at[b]
                 sides = (
                     (normed[:, :, cols].reshape(tokens, width), cols_in[0, k].reshape(tokens, width)),
                     (cots[:, :, cols].reshape(tokens, width), cols_in[1, k].reshape(tokens, width)),
@@ -374,14 +407,27 @@
                     out[j] = (one if j < 2 else 0.5 * one).astype(jnp.bfloat16)
                     if k == 1 and (b == 0 or j < 2):
                         grad_back(b, j).start()
+            keep_grads(b).start()
+
+        def keep_grads(b):
+            return local(own_grads.at[b], grads[b], 25 + b)
+
+        def keep_late(m):
+            at = own_quarter(column(m))
+            return local(late.at[1, m, pl.ds(0, q)], late_mid.at[at], 27 + m)
 
         def rows_grad(b, r, out):
-            for m in range(1, TP):
-                part_copy(b, r, m).wait_recv()
+            if b == 0:
+                copies = part_first(r, kinds=(0,)) + part_second(r)
+            else:
+                copies = [part_copy(r, m) for m in range(1, TP)]
+            for copy in copies:
+                copy.wait_recv()
             arrived = (part_in2, part_in1)[b]
-            at = part_rows(b, r)
+            size = half if b == 0 else q
+            at = pl.ds(r * size, size)
             total = part[0, at, :].astype(jnp.float32)
-            for m in range(1, TP):
+            for m in range(1, 3 if b == 0 else TP):
                 total = total + arrived[m - 1, at, :].astype(jnp.float32)
             wide, factor = norm_parts(acts[2 * b, 0, at, :])
             scaled = total * gains[b][...]
@@ -397,7 +443,19 @@
                 device(z, core, column(m)),
             )
 
-        def late_block(b, n, take):
+        def mid_forward(h, m):
+            at = pl.ds(h * half + (m - 1) * q, q)
+            return remote(
+                acts.at[3, m, at], acts.at[3, 3, at], sem(("f", h, m)),
+                device(z, core, column(3 - m)),
+            )
+
+        def mid_pass(h):
+            for m in (1, 2):
+                mid_copy(h, m).wait_recv()
+                mid_forward(h, m).start()
+
+        def late_block(b, n):
             @pl.loop(0, TP * 2)
             def _(i):
                 at = pl.ds(pl.multiple_of((i % 2) * q, q), q)
@@ -416,29 +474,53 @@
             gate = late_acc[0]
             hid = (gate / (1.0 + jnp.exp(-gate)) * late_acc[1]).astype(jnp.bfloat16)
             late_hid[...] = hid
-            if take:
-                take_down(b)
+            if n == 0:
+                late_acc[...] = jnp.zeros_like(late_acc)
+                for h in range(2):
+                    for m in (1, 2):
+                        mid_forward(h, m).wait_recv()
 
             @pl.loop(0, 8)
             def _(i):
-                cols = feature(i % 4, i // 4)
-                one = mm(late_hid[...], weights[b, i, parts[2], :], NN).astype(jnp.bfloat16)
+                slot, other = i // 2, i % 2
+                if n == 0:
+                    take_part(b, 2, slot, other)
+                cols = feature(slot, other)
+                w = weights[b, slot + 4 * other, parts[2], :]
+                one = mm(late_hid[...], w, NN).astype(jnp.bfloat16)
                 late_part[:, :, cols] = one.reshape(TP, half, width)
-
-            for r in (1, 0):
-                for m in range(1, TP):
-                    late_copy(n, r, m).start()
-
-        def late_copy(n, r, m):
+                if n == 0:
+                    for m in range(1, TP):
+                        late_block_copy(i, m).start()
+                    down_shard(b, slot, other)
+
+            if n == 1:
+                for r in (1, 0):
+                    for m in range(1, TP):
+                        late_copy(r, m).start()
+
+        late_base = sem(("b", 0))
+        for i in range(1, 24):
+            sem(("b", i))
+
+        def late_block_copy(i, m):
+            cols = feature(i // 2, i % 2)
+            return remote(
+                late_part.at[m, :, cols], late_part_in.at[0, m - 1, :, cols],
+                late_base + i * 3 + (m - 1), device(z, core, column(m)),
+            )
+
+        def late_copy(r, m):
             at = pl.ds(r * q, q)
             return remote(
-                late_part.at[m, at], late_part_in.at[n, m - 1, at], sem(("h", n, r, m)),
+                late_part.at[m, at], late_part_in.at[1, m - 1, at], sem(("h", r, m)),
                 device(z, core, column(m)),
             )
 
         def late_sum(n, r, out):
-            for m in range(1, TP):
-                late_copy(n, r, m).wait_recv()
+            if n == 1:
+                for m in range(1, TP):
+                    late_copy(r, m).wait_recv()
             at = pl.ds(r * q, q)
             total = late_part[0, at, :].astype(jnp.float32)
             for m in range(1, TP):
@@ -451,39 +533,45 @@
                 late.at[1, 0], late.at[1, m], sem(("k", m)), device(z, core, column(m))
             )
 
+        def late_forward(m):
+            at = pl.ds((m - 1) * q, q)
+            return remote(
+                late.at[1, m, at], late.at[1, 3, at], sem(("j", m)), device(z, core, column(3 - m))
+            )
+
         rows_ready(0)
         normalize_block(0)
-        pre_block(0)
+        pre_block(0, 0, 8)
         rows_ready(1)
         gather_rows(2, 4)
         gather_rows(3, 5)
-        down_block(0, True)
+        down_block(0)
         for h in range(2):
             pieces_block(h)
             grad_part(0, h)
-            for m in range(1, TP):
-                part_copy(0, h, m).start()
+            for copy in part_first(h):
+                copy.start()
         for copy in swaps(0):
             copy.start()
-        for h in range(2):
-            rows_grad(0, h, acts.at[3, 0])
-            for m in range(1, TP):
-                mid_copy(h, m).start()
-            if h == 0:
-                fold(0)
+        part_merge(0)
+        fold(0)
+        part_merge(1)
         for copy in swaps(0):
             copy.wait_send()
         pl.semaphore_signal(ack, inc=1, device_id=peer_dev, device_id_type=pl.DeviceIdType.MESH)
 
         rows_ready(2)
         normalize_block(1)
-        pre_block(1)
+        for h in range(2):
+            rows_grad(0, h, acts.at[3, 0])
+            for m in (1, 2):
+                mid_copy(h, m).start()
+            pre_block(1, 2 * h, 2 + 3 * h)
+        mid_pass(0)
+        mid_pass(1)
+        pre_block(1, 5, 8)
         rows_ready(3)
-        late_block(1, 0, True)
-        for h in range(2):
-            for m in range(1, TP):
-                mid_copy(h, m).wait_recv()
-        down_block(1, False)
+        late_block(1, 0)
 
         @pl.loop(0, 2)
         def _(h):
@@ -492,33 +580,46 @@
         pl.semaphore_wait(ack, 1)
         for copy in swaps(1):
             copy.start()
-        for r in range(2):
+
+        @pl.loop(0, 8)
+        def _(i):
             for m in range(1, TP):
-                part_copy(0, r, m).wait_send()
-        grad_part(1, 0)
+                late_block_copy(i, m).wait_recv()
+
         late_rows = late.at[1, 0]
         late_sum(0, 1, late_rows)
         late_sum(0, 0, late_rows)
-        for m in range(1, TP):
+        for m in (1, 2):
             late_spread(m).start()
         rows_back(0).start()
+        for h in range(2):
+            for copy in part_first(h) + part_second(h):
+                copy.wait_send()
+        grad_part(1, 0)
+        for m in (1, 2):
+            late_spread(m).wait_recv()
+            late_forward(m).start()
         for r in (1, 0):
             for m in range(1, TP):
-                part_copy(1, r, m).start()
+                part_copy(r, m).start()
         fold(1)
-        for m in range(1, TP):
-            late_spread(m).wait_recv()
-            for r in range(2):
-                late_copy(0, r, m).wait_send()
-        late_block(0, 1, False)
+
+        @pl.loop(0, 8)
+        def _(i):
+            for m in range(1, TP):
+                late_block_copy(i, m).wait_send()
+
+        for m in (1, 2):
+            late_forward(m).wait_recv()
+        late_block(0, 1)
         for m in range(TP):
-            late_mid[own_quarter(column(m)), :] = late[1, m, pl.ds(0, q), :]
+            keep_late(m).start()
 
         def finish(k):
             src = row_source(k).at[pl.ds(0, q)]
             for m in range(1, TP):
                 deliver(k, m, src).start()
-            out_rows[k][mine, :] = src[...]
+            keep_rows(k, src).start()
 
         rows_grad(1, 1, done_rows.at[1])
         rows_back(2).start()
@@ -545,13 +646,22 @@
             copy.wait_send()
         for m in range(1, TP):
             for r in range(2):
-                mid_copy(r, m).wait_send()
-                part_copy(1, r, m).wait_send()
-                late_copy(1, r, m).wait_send()
+                part_copy(r, m).wait_send()
+                late_copy(r, m).wait_send()
+        for m in (1, 2):
             late_spread(m).wait_send()
+            late_forward(m).wait_send()
+            for h in range(2):
+                mid_copy(h, m).wait_send()
+                mid_forward(h, m).wait_send()
+        for b in range(2):
+            keep_grads(b).wait()
+        for m in range(TP):
+            keep_late(m).wait()
         for k in range(3):
             rows_back(k).wait_send()
             if k > 0:
+                keep_rows(k, row_source(k).at[pl.ds(0, q)]).wait()
                 for m in range(1, TP):
                     deliver(k, m, row_source(k).at[pl.ds(0, q)]).wait_send()
                     deliver_wait(k, m)
@@ -595,7 +705,7 @@
         step_kernel,
         out_shape=[rows_shape] * 3 + [grads_shape] * 2,
         in_specs=[anywhere] * 4 + [in_vmem] * 2 + [anywhere] * 6,
-        out_specs=[in_vmem] * 5,
+        out_specs=[anywhere] * 5,
         scratch_shapes=[
             pltpu.VMEM((2, 8, 3 * hidden, width), bf),
             pltpu.VMEM((4, TP, count, feats), bf),
@@ -613,12 +723,13 @@
             pltpu.VMEM((2, 3, hidden, width), bf),
             pltpu.VMEM((3, q, feats), bf),
             pltpu.VMEM((2, half, feats), bf),
+            pltpu.VMEM((2, 3, hidden, width), bf),
             pltpu.VMEM((2, 2, tile, hidden), jnp.float32),
             pltpu.VMEM((2, tile, hidden), jnp.float32),
             pltpu.VMEM((tile, hidden), bf),
-            pltpu.SemaphoreType.DMA((160,)),
-            pltpu.SemaphoreType.DMA((160,)),
-            pltpu.SemaphoreType.DMA((22,)),
+            pltpu.SemaphoreType.DMA((208,)),
+            pltpu.SemaphoreType.DMA((208,)),
+            pltpu.SemaphoreType.DMA((31,)),
             pltpu.SemaphoreType.REGULAR,
         ],
         compiler_params=pltpu.CompilerParams(

time: 201 us -> 189 us (0.940)
  Pallas kernels: 197 us -> 185 us
    pallas_call x1, Pallas kernels: 191 us -> 179 us  [per_device(): pl.pallas_call(step_kernel, out_shape=[rows_shape] * 3 + [grads_shape] *...]
where the time goes in v3:
time: 189 us; the launch traced here: 186 us
  Pallas kernels  185 us (98%)
    pallas_call x1, Pallas kernels, per_device(): pl.pallas_call(step_kernel, out_shape=[rows_shape] * 3 + [grads_shape] *...  179 us
    pallas_call x1, Pallas kernels, per_device(): pl.pallas_call(add_kernel, grid=(steps,), out_shape=[rows_shape] * 3 + [j...  6.14 us

profile of v3, /device:TPU:0, one launch (start us, length us, event | category | flops | bytes accessed | tf_op | source)
XLA Modules:
  0.0 186.0 jit_solution(18216797028086767367)
XLA Ops:
  0.6 179.1 %step.1 = (bf16[128,2048]{1,0:T(8,128)(2,1)}, bf16[128,2048]{1,0:T(8,128)(2,1)}, bf16[128,2048]{1,0:T(8,128)(2,1)}, bf16[3,704,256]{2,1,0:T(8,128)(2,1)}, bf16[3,704,256]{2,1,0:T(8,128)(2,1)}) custom-call(bf16[128,2048]{1,0:T(8,128)(2,1)} %late_in.1, bf16[128,2048]{1,0:T(8,128)(2,1)} %mid_in.1, bf16[128,2048]{1,0:T(8,128)(2,1)} %cot_in.1, ...), custom_call_target="tpu_custom_call" | custom-call | tf_op jit(solution)/shard_map/step/pallas_call | solution.py:704
  179.7 6.1 %add.1 = (bf16[128,2048]{1,0:T(8,128)(2,1)}, bf16[128,2048]{1,0:T(8,128)(2,1)}, bf16[128,2048]{1,0:T(8,128)(2,1)}, f32[704,256]{1,0:T(8,128)}, f32[704,256]{1,0:...) custom-call(bf16[128,2048]{1,0:T(8,128)(2,1)} %get-tuple-element.23.r0, ...), custom_call_target="tpu_custom_call" | custom-call | tf_op jit(solution)/shard_map/add/pallas_call | solution.py:750

commit v4 on v3

--- a/solution.py
+++ b/solution.py
@@ -743,7 +743,7 @@
         gate_first.T, up_first.T, down_first,
     )
     tall = [old.T if j % 3 < 2 else old for j, old in enumerate(sums)]
-    steps = 4
+    steps = 2
     row_spec = pl.BlockSpec((count // steps, feats), lambda i: (i, 0))
     sum_spec = pl.BlockSpec((hidden // steps, width), lambda i: (i, 0))
     grad_spec = pl.BlockSpec((3, hidden // steps, width), lambda i: (0, i, 0))

time: 189 us -> 188 us (level)
  no operation moved by 1% of the time
where the time goes in v4:
time: 188 us; the launch traced here: 185 us
  Pallas kernels  184 us (98%)
    pallas_call x1, Pallas kernels, per_device(): pl.pallas_call(step_kernel, out_shape=[rows_shape] * 3 + [grads_shape] *...  179 us
    pallas_call x1, Pallas kernels, per_device(): pl.pallas_call(add_kernel, grid=(steps,), out_shape=[rows_shape] * 3 + [j...  5.23 us

profile of v4, /device:TPU:0, one launch (start us, length us, event | category | flops | bytes accessed | tf_op | source)
XLA Modules:
  0.0 185.1 jit_solution(3131685482729738731)
XLA Ops:
  0.6 179.1 %step.1 = (bf16[128,2048]{1,0:T(8,128)(2,1)}, bf16[128,2048]{1,0:T(8,128)(2,1)}, bf16[128,2048]{1,0:T(8,128)(2,1)}, bf16[3,704,256]{2,1,0:T(8,128)(2,1)}, bf16[3,704,256]{2,1,0:T(8,128)(2,1)}) custom-call(bf16[128,2048]{1,0:T(8,128)(2,1)} %late_in.1, bf16[128,2048]{1,0:T(8,128)(2,1)} %mid_in.1, bf16[128,2048]{1,0:T(8,128)(2,1)} %cot_in.1, ...), custom_call_target="tpu_custom_call" | custom-call | tf_op jit(solution)/shard_map/step/pallas_call | solution.py:704
  179.7 5.2 %add.1 = (bf16[128,2048]{1,0:T(8,128)(2,1)}, bf16[128,2048]{1,0:T(8,128)(2,1)}, bf16[128,2048]{1,0:T(8,128)(2,1)}, f32[704,256]{1,0:T(8,128)}, f32[704,256]{1,0:...) custom-call(bf16[128,2048]{1,0:T(8,128)(2,1)} %get-tuple-element.23.r0, ...), custom_call_target="tpu_custom_call" | custom-call | tf_op jit(solution)/shard_map/add/pallas_call | solution.py:750
